TPU v7x, 32 devices: a whole 2x2x4 slice. The times are simulated.
32 devices in a mesh: fs: 8 (over z, x), tp: 4 (over y, core).
Axes of the slice: x: 2, y: 2, z: 4, core: 2. Of those that a mesh axis runs over, the one named last changes fastest.
Arguments:
- late_input: bfloat16 [4096, 2048], P(('fs', 'tp')), may hold values from -6 to 6
- norm_gain: bfloat16 [2048], replicated, may hold values from 0.099609375 to 1.8984375
- gate_weight: bfloat16 [2048, 2816], P('fs', 'tp'), may hold values from -0.125 to 0.125
- up_weight: bfloat16 [2048, 2816], P('fs', 'tp'), may hold values from -0.125 to 0.125
- down_weight: bfloat16 [2048, 2816], P('fs', 'tp'), may hold values from -0.109375 to 0.109375
- early_input: bfloat16 [4096, 2048], P(('fs', 'tp')), may hold values from -6 to 6
- cotangent: bfloat16 [4096, 2048], P(('fs', 'tp')), may hold values from -6 to 6
- gate_sum: float32 [2048, 2816], P('fs', 'tp'), may hold values from -192 to 192
- up_sum: float32 [2048, 2816], P('fs', 'tp'), may hold values from -192 to 192
- down_sum: float32 [2048, 2816], P('fs', 'tp'), may hold values from -192 to 192
- gain_sum: float32 [2048], replicated, may hold values from -192 to 192
Outputs:
- late_out: bfloat16 [4096, 2048], P(('fs', 'tp'))
- early_grad: bfloat16 [4096, 2048], P(('fs', 'tp'))
- gate_sum_out: float32 [2048, 2816], P('fs', 'tp')
- up_sum_out: float32 [2048, 2816], P('fs', 'tp')
- down_sum_out: float32 [2048, 2816], P('fs', 'tp')
- gain_sum_out: float32 [2048], replicated
All inputs are finite; a program needn't handle non-finite values.
Results may differ from a plain program's by a relative error of at most 0.008.
Values may be sent and summed in bfloat16 or wider, within the bound.
A program may use at most 128 MiB of HBM per device.

v0:
```python
import jax
import jax.numpy as jnp
from jax import lax
from jax.sharding import PartitionSpec as P

epsilon = 1e-05


def normalize(source, gain_f):
    values = source.astype(jnp.float32)
    scale = lax.rsqrt(jnp.mean(values * values, axis=-1, keepdims=True) + epsilon)
    return ((values * scale * gain_f).astype(jnp.bfloat16), scale, values)


def times_transposed(left, right):
    return lax.dot_general(
        left, right, (((1,), (1,)), ((), ())), preferred_element_type=jnp.float32
    )


def column_product(left, right):
    return lax.dot_general(
        left, right, (((0,), (0,)), ((), ())), preferred_element_type=jnp.float32
    )


def per_device(
    late_input,
    norm_gain,
    gate_weight,
    up_weight,
    down_weight,
    early_input,
    cotangent,
    gate_sum,
    up_sum,
    down_sum,
    gain_sum,
):
    gate_whole, up_whole, down_whole = (
        lax.all_gather(gate_weight, "fs", axis=0, tiled=True),
        lax.all_gather(up_weight, "fs", axis=0, tiled=True),
        lax.all_gather(down_weight, "fs", axis=0, tiled=True),
    )
    gain_f = norm_gain.astype(jnp.float32)
    width = gate_weight.shape[1]
    normed, scale, values = normalize(late_input, gain_f)
    piece = lax.all_gather(normed, "tp", axis=0, tiled=True)
    gate = jnp.dot(piece, gate_whole, preferred_element_type=jnp.float32)
    upper = jnp.dot(piece, up_whole, preferred_element_type=jnp.float32)
    hidden = (jax.nn.silu(gate) * upper).astype(jnp.bfloat16)
    mixed = lax.psum_scatter(
        times_transposed(hidden, down_whole).astype(jnp.bfloat16),
        "tp",
        scatter_dimension=0,
        tiled=True,
    ).astype(jnp.float32)
    late_out = (values + 0.5 * mixed).astype(jnp.bfloat16)
    normed_e, scale_e, values_e = normalize(early_input, gain_f)
    normed_all = lax.all_gather(normed_e, "tp", axis=0, tiled=True)
    cot_all = lax.all_gather(cotangent, "tp", axis=0, tiled=True)
    gate_e = jnp.dot(normed_all, gate_whole, preferred_element_type=jnp.float32)
    upper_e = jnp.dot(normed_all, up_whole, preferred_element_type=jnp.float32)
    sigma_e = jax.nn.sigmoid(gate_e)
    hidden_e = (gate_e * sigma_e * upper_e).astype(jnp.bfloat16)
    d_hidden = 0.5 * jnp.dot(cot_all, down_whole, preferred_element_type=jnp.float32)
    d_gate = (d_hidden * upper_e * sigma_e * (1.0 + gate_e * (1.0 - sigma_e))).astype(jnp.bfloat16)
    d_up = (d_hidden * gate_e * sigma_e).astype(jnp.bfloat16)
    d_normed = lax.psum_scatter(
        (times_transposed(d_gate, gate_whole) + times_transposed(d_up, up_whole)).astype(
            jnp.bfloat16
        ),
        "tp",
        scatter_dimension=0,
        tiled=True,
    ).astype(jnp.float32)
    scaled_grad = d_normed * gain_f
    early_grad = (
        cotangent.astype(jnp.float32)
        + scale_e * scaled_grad
        - values_e * scale_e**3 * jnp.mean(values_e * scaled_grad, axis=-1, keepdims=True)
    ).astype(jnp.bfloat16)
    gain_part = jnp.sum(d_normed * values_e * scale_e, axis=0)
    gain_sum_out = gain_sum + lax.psum(gain_part, ("fs", "tp"))
    summed = lax.psum_scatter(
        jnp.concatenate(
            [
                column_product(normed_all, d_gate),
                column_product(normed_all, d_up),
                0.5 * column_product(cot_all, hidden_e),
            ],
            axis=1,
        ),
        "fs",
        scatter_dimension=0,
        tiled=True,
    )
    gate_grad = summed[:, :width]
    up_grad = summed[:, width : 2 * width]
    down_grad = summed[:, 2 * width :]
    early_grad, gate_sum_out, up_sum_out, down_sum_out, gain_sum_out = (
        early_grad,
        gate_sum + gate_grad,
        up_sum + up_grad,
        down_sum + down_grad,
        gain_sum_out,
    )
    return (late_out, early_grad, gate_sum_out, up_sum_out, down_sum_out, gain_sum_out)


def solution(mesh):
    placed = (
        P(("fs", "tp"), None),
        P(),
        P("fs", "tp"),
        P("fs", "tp"),
        P("fs", "tp"),
        P(("fs", "tp"), None),
        P(("fs", "tp"), None),
        P("fs", "tp"),
        P("fs", "tp"),
        P("fs", "tp"),
        P(),
    )
    return jax.shard_map(
        per_device,
        mesh=mesh,
        in_specs=placed,
        out_specs=(
            P(("fs", "tp"), None),
            P(("fs", "tp"), None),
            P("fs", "tp"),
            P("fs", "tp"),
            P("fs", "tp"),
            P(),
        ),
        check_vma=False,
    )
```

profile of v0, /device:TPU:0, one launch (start us, length us, event | category | flops | bytes accessed | tf_op | source)
XLA Modules:
  0.0 657.0 jit_solution(9303688887401447348)
XLA Ops:
  7.2 1.2 fusion.9
  8.5 0.7 convert_element_type.49
  9.1 2.0 fusion.11
  11.2 0.7 all-gather.9.cloned.1.call-update
  12.0 0.7 all-gather.11.cloned.1.call-update
  13.9 22.7 %all-gather.17.cloned.1.call-done = bf16[512,2048]{1,0:T(8,128)(2,1)} async-done(((bf16[128,2048]{1,0:T(8,128)(2,1)}), bf16[512,2048]{1,0:T(8,128)(2,1)}) %all-gather.17.cloned.1.call-update) | async-done | bytes 2097168 | tf_op jit(solution)/shard_map/all_gather | solution.py:60
  36.6 61.6 %all-gather.9.cloned.1.call-done = bf16[2048,704]{0,1:T(8,128)(2,1)} async-done(((bf16[256,704]{0,1:T(8,128)(2,1)}), bf16[2048,704]{0,1:T(8,128)(2,1)}) %all-gather.9.cloned.1.call-update) | async-done | bytes 2883600 | tf_op jit(solution)/shard_map/all_gather | solution.py:41
  98.3 5.2 fusion.21
  103.5 54.6 %all-gather.11.cloned.1.call-done = bf16[2048,704]{0,1:T(8,128)(2,1)} async-done(((bf16[256,704]{0,1:T(8,128)(2,1)}), bf16[2048,704]{0,1:T(8,128)(2,1)}) %all-gather.11.cloned.1.call-update) | async-done | bytes 2883600 | tf_op jit(solution)/shard_map/all_gather | solution.py:42
  158.1 4.6 fusion.20
  162.7 17.6 %all-gather.15.cloned.1.call-done = bf16[512,2048]{1,0:T(8,128)(2,1)} async-done(((bf16[128,2048]{1,0:T(8,128)(2,1)}), bf16[512,2048]{1,0:T(8,128)(2,1)}) %all-gather.15.cloned.1.call-update) | async-done | bytes 2097168 | tf_op jit(solution)/shard_map/all_gather | solution.py:61
  180.3 61.5 %all-gather.13.cloned.1.call-done = bf16[2048,704]{0,1:T(8,128)(2,1)} async-done(((bf16[256,704]{0,1:T(8,128)(2,1)}), bf16[2048,704]{0,1:T(8,128)(2,1)}) %all-gather.13.cloned.1.call-update) | async-done | bytes 2883600 | tf_op jit(solution)/shard_map/all_gather | solution.py:43
  241.8 5.5 multiply_convert_fusion.1
  247.4 1.8 fusion.22
  249.7 3.4 add_convert_fusion
  253.1 1.0 copy-done.2
  254.3 28.3 %reduce-scatter.6.cloned.1.call-done = bf16[128,2048]{1,0:T(8,128)(2,1)} async-done(((bf16[512,2048]{1,0:T(8,128)(2,1)}), bf16[128,2048]{1,0:T(8,128)(2,1)}) %reduce-scatter.6.cloned.1.call-update) | async-done | bytes 524304 | tf_op jit(solution)/shard_map/reduce_scatter | solution.py:69
  282.6 1.4 fusion.15
  284.0 2.7 fusion.4
  286.9 22.5 %all-gather.7.cloned.1.call-done = bf16[512,2048]{1,0:T(8,128)(2,1)} async-done(((bf16[128,2048]{1,0:T(8,128)(2,1)}), bf16[512,2048]{1,0:T(8,128)(2,1)}) %all-gather.7.cloned.1.call-update) | async-done | bytes 2097168 | tf_op jit(solution)/shard_map/all_gather | solution.py:48
  309.4 5.2 fusion.19
  314.6 8.6 %convolution_convert_fusion = bf16[512,2048]{1,0:T(8,128)(2,1)} fusion(bf16[2048,704]{0,1:T(8,128)(2,1)} %all-gather.13.cloned.1.call-done, bf16[512,2048]{1,0:T(8,128)(2,1)} %all-gather.7.cloned.1.call-done, bf16[2048,704]{0,1:T(8,128)(2,1)} %all-gather.11.cloned.1.call-done, f32[512,704]{0,1:T(8,128)} %fusion.19), kind=kOutput, calls=%fused_computation.3 | convolution fusion | flops 2956001280 | bytes 11403264 | tf_op jit(solution)/shard_map/dot_general | solution.py:16
  323.3 1.0 copy-done.7
  324.3 1.7 fusion.24
  326.0 1.7 fusion.23
  328.4 1.7 multiply_bitcast_fusion
  330.1 6.6 pad_maximum_fusion
  336.7 40.6 %psum.7 = f32[2048]{0:T(1024)S(1)} all-reduce(f32[2048]{0:T(1024)S(1)} %get-tuple-element.6), channel_id=1, replica_groups=mesh['fs'=8,'tp'=4] {'fs','tp'}, use_global_device_ids=true, to_apply=%region_7.8 | all-reduce | flops 2048 | bytes 16384 | tf_op jit(solution)/shard_map/psum | solution.py:84
  377.3 0.6 add.69
  377.9 2.0 fusion.8
  379.9 267.6 %reduce-scatter.8.cloned.1.call-done = f32[256,2112]{0,1:T(8,128)} async-done(((f32[2048,2112]{0,1:T(8,128)}), f32[256,2112]{0,1:T(8,128)}) %reduce-scatter.8.cloned.1.call-update) | async-done | bytes 2162704 | tf_op jit(solution)/shard_map/reduce_scatter | solution.py:85
  647.5 3.0 slice_add_fusion
  (51 shorter events, 3.1 us)
Async XLA Ops:
  7.2 29.5 %all-gather.17.cloned.1.call-start = ((), (), s32[]{:S(2)}) async-start(), calls=%async_computation.9 | async-start | bytes 2621440 | tf_op jit(solution)/shard_map/all_gather | solution.py:60
  11.2 87.1 %all-gather.9.cloned.1.call-start = ((), (), s32[]{:S(2)}) async-start(), calls=%async_computation.4 | async-start | bytes 3244032 | tf_op jit(solution)/shard_map/all_gather | solution.py:41
  11.9 146.1 %all-gather.11.cloned.1.call-start = ((), (), s32[]{:S(2)}) async-start(), calls=%async_computation.5 | async-start | bytes 3244032 | tf_op jit(solution)/shard_map/all_gather | solution.py:42
  12.7 167.6 %all-gather.15.cloned.1.call-start = ((), (), s32[]{:S(2)}) async-start(), calls=%async_computation.8 | async-start | bytes 2621440 | tf_op jit(solution)/shard_map/all_gather | solution.py:61
  13.3 228.5 %all-gather.13.cloned.1.call-start = ((), (), s32[]{:S(2)}) async-start(), calls=%async_computation.6 | async-start | bytes 3244032 | tf_op jit(solution)/shard_map/all_gather | solution.py:43
  13.8 268.8 %reduce-scatter.6.cloned.1.call-start = ((), (), s32[]{:S(2)}) async-start(), calls=%async_computation.10 | async-start | bytes 2621440 | tf_op jit(solution)/shard_map/reduce_scatter | solution.py:69
  36.6 121.5 %copy-start.1 = (bf16[512,2048]{1,0:T(8,128)(2,1)S(1)}, bf16[512,2048]{1,0:T(8,128)(2,1)}, u32[]{:S(2)}) copy-start(bf16[512,2048]{1,0:T(8,128)(2,1)} %all-gather.17.cloned.1.call-done) | copy-start | bytes 6291460
  241.8 5.6 copy-start.5
  247.3 1.9 copy-start.3
  247.3 1.9 copy-start.6
  247.4 2.3 copy-start.12
  253.1 1.0 copy-start.2
  253.1 29.5 %copy-start = (bf16[128,2048]{1,0:T(8,128)(2,1)S(1)}, bf16[128,2048]{1,0:T(8,128)(2,1)}, u32[]{:S(2)}) copy-start(bf16[128,2048]{1,0:T(8,128)(2,1)} %param.16) | copy-start | bytes 1572868
  253.1 56.3 %all-gather.7.cloned.1.call-start = ((), (), s32[]{:S(2)}) async-start(), calls=%async_computation.3 | async-start | bytes 2621440 | tf_op jit(solution)/shard_map/all_gather | solution.py:48
  286.7 91.2 %reduce-scatter.4.cloned.1.call-start = ((), (), s32[]{:S(2)}) async-start(), calls=%async_computation.7 | async-start | bytes 2621440 | tf_op jit(solution)/shard_map/reduce_scatter | solution.py:52
  323.2 1.1 copy-start.7
  323.2 324.3 %reduce-scatter.8.cloned.1.call-start = ((), (), s32[]{:S(2)}) async-start(), calls=%async_computation.11 | async-start | bytes 19464192 | tf_op jit(solution)/shard_map/reduce_scatter | solution.py:85
  324.3 1.7 copy-start.4
  326.0 1.7 copy-start.13
  326.0 2.0 copy-start.14
  326.0 2.4 copy-start.15
  336.7 40.6 %copy-start.11 = (f32[2048]{0:T(1024)S(1)}, f32[2048]{0:T(1024)}, u32[]{:S(2)}) copy-start(f32[2048]{0:T(1024)} %param.21) | copy-start | bytes 24580
  336.7 310.8 %copy-start.10 = (f32[256,704]{0,1:T(8,128)S(1)}, f32[256,704]{0,1:T(8,128)}, u32[]{:S(2)}) copy-start(f32[256,704]{0,1:T(8,128)} %param.18) | copy-start | bytes 2162692
  336.7 310.8 %copy-start.8 = (f32[256,704]{0,1:T(8,128)S(1)}, f32[256,704]{0,1:T(8,128)}, u32[]{:S(2)}) copy-start(f32[256,704]{0,1:T(8,128)} %param.20) | copy-start | bytes 2162692
  336.7 310.8 %copy-start.9 = (f32[256,704]{0,1:T(8,128)S(1)}, f32[256,704]{0,1:T(8,128)}, u32[]{:S(2)}) copy-start(f32[256,704]{0,1:T(8,128)} %param.19) | copy-start | bytes 2162692
Sparse Core Ops, SparseCore 0:
  11.3 25.2 all-gather.16
  38.7 59.5 all-gather.8
  100.3 57.7 all-gather.10
  159.5 20.7 all-gather.14
  182.2 59.5 all-gather.12
  253.2 29.3 reduce-scatter.5
  286.8 22.5 all-gather.6
  323.3 31.8 reduce-scatter.3
  359.2 288.2 reduce-scatter.7
where the time goes:
time: 658 us; the launch traced here: 657 us
  waiting for transfers between devices  539 us (82%)
  blocking collectives  40.6 us (6%)
  matrix products  39.4 us (6%)
  other arithmetic  20.3 us (3%)
  between operations  14 us (2%)
    reduce_scatter x1, waiting for transfers between devices, per_device(): lax.psum_scatter(jnp.concatenate([column_product(normed_all, d_gate), col...  268 us
    all_gather x1, waiting for transfers between devices, per_device(): lax.all_gather(gate_weight, 'fs', axis=0, tiled=True)  61.6 us
    all_gather x1, waiting for transfers between devices, per_device(): lax.all_gather(down_weight, 'fs', axis=0, tiled=True)  61.5 us
    all_gather x1, waiting for transfers between devices, per_device(): lax.all_gather(up_weight, 'fs', axis=0, tiled=True)  54.6 us
    psum x1, blocking collectives, per_device(): gain_sum_out = gain_sum + lax.psum(gain_part, ('fs', 'tp'))  40.6 us
    reduce_scatter x1, waiting for transfers between devices, per_device(): lax.psum_scatter((times_transposed(d_gate, gate_whole) + times_transposed...  28.3 us
    all_gather x1, waiting for transfers between devices, per_device(): normed_all = lax.all_gather(normed_e, 'tp', axis=0, tiled=True)  22.7 us
    all_gather x1, waiting for transfers between devices, per_device(): piece = lax.all_gather(normed, 'tp', axis=0, tiled=True)  22.5 us
  transfers between devices with their start and end apart: 9, of which 8 were waited for; matrix products, arithmetic and copies ran while one was open for 4% of the time, Pallas kernels for 0%

commit v1 on v0

v1 whole, which is shorter than its diff:
```python
import functools

import jax
import jax.numpy as jnp
from jax import lax
from jax.experimental import pallas as pl
from jax.experimental.pallas import tpu as pltpu
from jax.sharding import PartitionSpec as P

epsilon = 1e-05
MESH = pl.DeviceIdType.MESH
VMEM_LIMIT = 60 * 1024 * 1024


def ring_place(index, n):
    odd = lax.rem(index, 2)
    half = index // 2
    return (1 - odd) * half + odd * (n - 1 - half)


def ring_index(place, n):
    back = place // (n // 2)
    return (1 - back) * (2 * place) + back * (2 * (n - 1 - place) + 1)


def neighbours(n):
    place = ring_place(lax.axis_index("fs"), n)
    right = ring_index(lax.rem(place + 1, n), n)
    left = ring_index(lax.rem(place + n - 1, n), n)
    return place, right, left


def greet(n_tp, right, left):
    me_tp = lax.axis_index("tp")
    barrier = pltpu.get_barrier_semaphore()
    for target in (right, left):
        pl.semaphore_signal(barrier, inc=1, device_id=(target, me_tp), device_id_type=MESH)
    for away in range(1, n_tp):
        peer = lax.rem(me_tp + away, n_tp)
        pl.semaphore_signal(
            barrier, inc=1, device_id=(lax.axis_index("fs"), peer), device_id_type=MESH
        )
    pl.semaphore_wait(barrier, 2 + n_tp - 1)


def gather_kernel(n, n_tp, *refs):
    gu_ref, dn_ref, late_ref, early_ref, cot_ref = refs[:5]
    gu_all, dn_all, late_all, early_all, cot_all = refs[5:10]
    send_sem, recv_sem, tp_send, tp_recv, own_sem = refs[10:]
    me_fs, me_tp = lax.axis_index("fs"), lax.axis_index("tp")
    place, right, left = neighbours(n)
    greet(n_tp, right, left)
    rows = gu_ref.shape[0]
    half = rows // 2
    tokens = late_ref.shape[0]
    pairs = ((gu_ref, gu_all), (dn_ref, dn_all))

    def window(owner, way):
        return pl.ds(pl.multiple_of(owner * rows + way * half, half), half)

    def piece(step, c, way, first):
        block, whole = pairs[c]
        if way == 0:
            owner = ring_index(lax.rem(place - step + n, n), n)
            target = right
        else:
            owner = ring_index(lax.rem(place + step, n), n)
            target = left
        spot = whole.at[window(owner, way)]
        source = block.at[pl.ds(way * half, half)] if first else spot
        return pltpu.make_async_remote_copy(
            src_ref=source,
            dst_ref=spot,
            send_sem=send_sem.at[step, c, way],
            recv_sem=recv_sem.at[step, c, way],
            device_id=(target, me_tp),
            device_id_type=MESH,
        )

    for c in range(2):
        for way in range(2):
            piece(0, c, way, True).start()

    token_pairs = ((early_ref, early_all), (cot_ref, cot_all), (late_ref, late_all))
    token_copies = []
    for a, (block, whole) in enumerate(token_pairs):
        for away in range(1, n_tp):
            peer = lax.rem(me_tp + away, n_tp)
            copy = pltpu.make_async_remote_copy(
                src_ref=block,
                dst_ref=whole.at[pl.ds(pl.multiple_of(me_tp * tokens, tokens), tokens)],
                send_sem=tp_send.at[a, away - 1],
                recv_sem=tp_recv.at[a, away - 1],
                device_id=(me_fs, peer),
                device_id_type=MESH,
            )
            copy.start()
            token_copies.append(copy)
    own = []
    for a, (block, whole) in enumerate(token_pairs):
        own.append(
            pltpu.make_async_copy(
                block,
                whole.at[pl.ds(pl.multiple_of(me_tp * tokens, tokens), tokens)],
                own_sem.at[a],
            )
        )
    for c, (block, whole) in enumerate(pairs):
        own.append(
            pltpu.make_async_copy(
                block,
                whole.at[pl.ds(pl.multiple_of(me_fs * rows, rows), rows)],
                own_sem.at[3 + c],
            )
        )
    for copy in own:
        copy.start()

    def body(step, carry):
        for c in range(2):
            for way in range(2):
                piece(step - 1, c, way, False).wait_recv()
                piece(step, c, way, False).start()
        return carry

    lax.fori_loop(1, n - 1, body, 0)
    for c in range(2):
        for way in range(2):
            piece(n - 2, c, way, False).wait_recv()
            piece(0, c, way, True).wait_send()

    def drain(step, carry):
        for c in range(2):
            for way in range(2):
                piece(step, c, way, False).wait_send()
        return carry

    lax.fori_loop(1, n - 1, drain, 0)
    for copy in own:
        copy.wait()
    for copy in token_copies:
        copy.wait()


def gather(n, n_tp, gu, dn, late, early, cot):
    rows, width2 = gu.shape
    tokens, depth = late.shape
    vmem = pl.BlockSpec(memory_space=pltpu.VMEM)
    hbm = pl.BlockSpec(memory_space=pl.ANY)
    bf16 = jnp.bfloat16
    return pl.pallas_call(
        functools.partial(gather_kernel, n, n_tp),
        out_shape=[
            jax.ShapeDtypeStruct((n * rows, width2), bf16),
            jax.ShapeDtypeStruct((n * rows, dn.shape[1]), bf16),
        ]
        + [jax.ShapeDtypeStruct((n_tp * tokens, depth), bf16)] * 3,
        in_specs=[vmem] * 5,
        out_specs=[hbm] * 5,
        scratch_shapes=[
            pltpu.SemaphoreType.DMA((n - 1, 2, 2)),
            pltpu.SemaphoreType.DMA((n - 1, 2, 2)),
            pltpu.SemaphoreType.DMA((3, n_tp - 1)),
            pltpu.SemaphoreType.DMA((3, n_tp - 1)),
            pltpu.SemaphoreType.DMA((5,)),
        ],
        compiler_params=pltpu.CompilerParams(
            collective_id=0, has_side_effects=True, vmem_limit_bytes=VMEM_LIMIT
        ),
    )(gu, dn, late, early, cot)


def reduce_kernel(n, n_tp, *refs):
    gu_ref, dn_ref, mix_ref, dnorm_ref, gain_ref = refs[:5]
    gu_out, dn_out, mix_out, dnorm_out, gain_out = refs[5:10]
    (gu_slots, dn_slots, gain_slots, gain_tp) = refs[10:14]
    send_sem, recv_sem, gain_send, gain_recv, tp_send, tp_recv, last_send, last_recv = refs[14:]
    me_fs, me_tp = lax.axis_index("fs"), lax.axis_index("tp")
    place, right, left = neighbours(n)
    greet(n_tp, right, left)
    rows = gu_ref.shape[0] // n
    half = rows // 2
    tokens = mix_ref.shape[0] // n_tp
    sets = ((gu_ref, gu_slots, gu_out), (dn_ref, dn_slots, dn_out))

    def local(step, way):
        if way == 0:
            owner = ring_index(lax.rem(place - step - 1 + n, n), n)
        else:
            owner = ring_index(lax.rem(place + step + 1, n), n)
        return pl.ds(pl.multiple_of(owner * rows + way * half, half), half)

    def piece(step, c, way, first, landed=False):
        partial, slots, _ = sets[c]
        source = partial.at[local(0, way)] if first else slots.at[way, step if landed else step - 1]
        return pltpu.make_async_remote_copy(
            src_ref=source,
            dst_ref=slots.at[way, step],
            send_sem=send_sem.at[step, c, way],
            recv_sem=recv_sem.at[step, c, way],
            device_id=((left if way else right), me_tp),
            device_id_type=MESH,
        )

    def gain_piece(step):
        return pltpu.make_async_remote_copy(
            src_ref=gain_slots.at[ring_index(lax.rem(place - step + n, n), n)],
            dst_ref=gain_slots.at[ring_index(lax.rem(place - step + n, n), n)],
            send_sem=gain_send.at[step],
            recv_sem=gain_recv.at[step],
            device_id=(right, me_tp),
            device_id_type=MESH,
        )

    gain_slots[me_fs] = gain_ref[...]
    for c in range(2):
        for way in range(2):
            piece(0, c, way, True).start()
    tp_copies = []
    for a, (source, target) in enumerate(((dnorm_ref, dnorm_out), (mix_ref, mix_out))):
        for away in range(1, n_tp):
            peer = lax.rem(me_tp + away, n_tp)
            copy = pltpu.make_async_remote_copy(
                src_ref=source.at[pl.ds(pl.multiple_of(peer * tokens, tokens), tokens)],
                dst_ref=target.at[away - 1],
                send_sem=tp_send.at[a, away - 1],
                recv_sem=tp_recv.at[a, away - 1],
                device_id=(me_fs, peer),
                device_id_type=MESH,
            )
            copy.start()
            tp_copies.append(copy)
    gain_piece(0).start()

    def body(step, carry):
        for c in range(2):
            partial, slots, _ = sets[c]
            for way in range(2):
                piece(step - 1, c, way, False, True).wait_recv()
                slots[way, step - 1] = (
                    slots[way, step - 1].astype(jnp.float32)
                    + partial[local(step, way), :].astype(jnp.float32)
                ).astype(jnp.bfloat16)
                piece(step, c, way, False).start()
        gain_piece(step - 1).wait_recv()
        gain_piece(step).start()
        return carry

    lax.fori_loop(1, n - 1, body, 0)
    gain_piece(n - 2).wait_recv()
    total = gain_slots[0]
    for k in range(1, n):
        total = total + gain_slots[k]
    gain_tp[me_tp] = total
    last = []
    for away in range(1, n_tp):
        peer = lax.rem(me_tp + away, n_tp)
        copy = pltpu.make_async_remote_copy(
            src_ref=gain_tp.at[me_tp],
            dst_ref=gain_tp.at[me_tp],
            send_sem=last_send.at[away - 1],
            recv_sem=last_recv.at[away - 1],
            device_id=(me_fs, peer),
            device_id_type=MESH,
        )
        copy.start()
        last.append(copy)
    for c in range(2):
        partial, slots, out = sets[c]
        for way in range(2):
            piece(n - 2, c, way, False, True).wait_recv()
            out[pl.ds(way * half, half), :] = slots[way, n - 2].astype(jnp.float32) + partial[
                local(n - 1, way), :
            ].astype(jnp.float32)
            piece(0, c, way, True).wait_send()
    for copy in last:
        copy.wait()
    total = gain_tp[0]
    for k in range(1, n_tp):
        total = total + gain_tp[k]
    gain_out[...] = total

    def drain(step, carry):
        for c in range(2):
            for way in range(2):
                piece(step, c, way, False).wait_send()
        gain_piece(step).wait_send()
        return carry

    gain_piece(0).wait_send()
    lax.fori_loop(1, n - 1, drain, 0)
    for copy in tp_copies:
        copy.wait()


def reduce(n, n_tp, gu, dn, mix, dnorm, gain):
    rows = gu.shape[0] // n
    half = rows // 2
    tokens = mix.shape[0] // n_tp
    vmem = pl.BlockSpec(memory_space=pltpu.VMEM)
    hbm = pl.BlockSpec(memory_space=pl.ANY)
    f32, bf16 = jnp.float32, jnp.bfloat16
    return pl.pallas_call(
        functools.partial(reduce_kernel, n, n_tp),
        out_shape=[
            jax.ShapeDtypeStruct((rows, gu.shape[1]), f32),
            jax.ShapeDtypeStruct((rows, dn.shape[1]), f32),
            jax.ShapeDtypeStruct((n_tp - 1, tokens, mix.shape[1]), bf16),
            jax.ShapeDtypeStruct((n_tp - 1, tokens, mix.shape[1]), bf16),
            jax.ShapeDtypeStruct(gain.shape, f32),
        ],
        in_specs=[vmem, vmem, hbm, hbm, vmem],
        out_specs=[vmem, vmem, hbm, hbm, vmem],
        scratch_shapes=[
            pltpu.VMEM((2, n - 1, half, gu.shape[1]), bf16),
            pltpu.VMEM((2, n - 1, half, dn.shape[1]), bf16),
            pltpu.VMEM((n,) + gain.shape, f32),
            pltpu.VMEM((n_tp,) + gain.shape, f32),
            pltpu.SemaphoreType.DMA((n - 1, 2, 2)),
            pltpu.SemaphoreType.DMA((n - 1, 2, 2)),
            pltpu.SemaphoreType.DMA((n - 1,)),
            pltpu.SemaphoreType.DMA((n - 1,)),
            pltpu.SemaphoreType.DMA((2, n_tp - 1)),
            pltpu.SemaphoreType.DMA((2, n_tp - 1)),
            pltpu.SemaphoreType.DMA((n_tp - 1,)),
            pltpu.SemaphoreType.DMA((n_tp - 1,)),
        ],
        compiler_params=pltpu.CompilerParams(
            collective_id=1, has_side_effects=True, vmem_limit_bytes=VMEM_LIMIT
        ),
    )(gu, dn, mix, dnorm, gain)


def normalize(source, gain_f):
    values = source.astype(jnp.float32)
    scale = lax.rsqrt(jnp.mean(values * values, axis=-1, keepdims=True) + epsilon)
    return ((values * scale * gain_f).astype(jnp.bfloat16), scale, values)


def times_transposed(left, right):
    return lax.dot_general(
        left, right, (((1,), (1,)), ((), ())), preferred_element_type=jnp.float32
    )


def column_product(left, right):
    return lax.dot_general(
        left, right, (((0,), (0,)), ((), ())), preferred_element_type=jnp.float32
    )


def per_device(
    n,
    n_tp,
    late_input,
    norm_gain,
    gate_weight,
    up_weight,
    down_weight,
    early_input,
    cotangent,
    gate_sum,
    up_sum,
    down_sum,
    gain_sum,
):
    gain_f = norm_gain.astype(jnp.float32)
    width = gate_weight.shape[1]
    depth = late_input.shape[1]
    tokens = late_input.shape[0]
    normed, _, values = normalize(late_input, gain_f)
    normed_e, scale_e, values_e = normalize(early_input, gain_f)
    gu = jnp.concatenate([gate_weight, up_weight], axis=1)
    gu_all, down_all, late_all, early_all, cot_all = gather(
        n, n_tp, gu, down_weight, normed, normed_e, cotangent
    )
    both_e = jnp.dot(early_all, gu_all, preferred_element_type=jnp.float32)
    gate_e, upper_e = both_e[:, :width], both_e[:, width:]
    sigma_e = jax.nn.sigmoid(gate_e)
    hidden_e = (gate_e * sigma_e * upper_e).astype(jnp.bfloat16)
    d_hidden = 0.5 * jnp.dot(cot_all, down_all, preferred_element_type=jnp.float32)
    d_gate = (d_hidden * upper_e * sigma_e * (1.0 + gate_e * (1.0 - sigma_e))).astype(jnp.bfloat16)
    d_up = (d_hidden * gate_e * sigma_e).astype(jnp.bfloat16)
    d_both = jnp.concatenate([d_gate, d_up], axis=1)
    d_part = times_transposed(d_both, gu_all).astype(jnp.bfloat16)
    gain_part = (
        jnp.sum(d_part.astype(jnp.float32) * early_all.astype(jnp.float32), axis=0) / gain_f
    )
    gu_part = column_product(early_all, d_both).astype(jnp.bfloat16)
    down_part = (0.5 * column_product(cot_all, hidden_e)).astype(jnp.bfloat16)
    both = jnp.dot(late_all, gu_all, preferred_element_type=jnp.float32)
    hidden = (jax.nn.silu(both[:, :width]) * both[:, width:]).astype(jnp.bfloat16)
    mix_part = times_transposed(hidden, down_all).astype(jnp.bfloat16)
    gu_grad, down_grad, mix_got, d_got, gain_total = reduce(
        n, n_tp, gu_part, down_part, mix_part, d_part, gain_part.reshape(8, depth // 8)
    )
    start = lax.axis_index("tp") * tokens

    def gathered(part, got):
        total = lax.dynamic_slice_in_dim(part, start, tokens, 0).astype(jnp.float32)
        for k in range(n_tp - 1):
            total = total + got[k].astype(jnp.float32)
        return total

    late_out = (values + 0.5 * gathered(mix_part, mix_got)).astype(jnp.bfloat16)
    scaled_grad = gathered(d_part, d_got) * gain_f
    early_grad = (
        cotangent.astype(jnp.float32)
        + scale_e * scaled_grad
        - values_e * scale_e**3 * jnp.mean(values_e * scaled_grad, axis=-1, keepdims=True)
    ).astype(jnp.bfloat16)
    return (
        late_out,
        early_grad,
        gate_sum + gu_grad[:, :width],
        up_sum + gu_grad[:, width:],
        down_sum + down_grad,
        gain_sum + gain_total.reshape(depth),
    )


def solution(mesh):
    token = P(("fs", "tp"), None)
    weight = P("fs", "tp")
    return jax.shard_map(
        functools.partial(per_device, mesh.shape["fs"], mesh.shape["tp"]),
        mesh=mesh,
        in_specs=(token, P(), weight, weight, weight, token, token, weight, weight, weight, P()),
        out_specs=(token, token, weight, weight, weight, P()),
        check_vma=False,
    )
```

time: 658 us -> 250 us (0.38)
  waiting for transfers between devices: 539 us -> 0 us
  Pallas kernels: 0 us -> 188 us
  blocking collectives: 40.6 us -> 0 us
  between operations: 14 us -> 0.88 us
  local copies, waits for them, and re-layouts: 3.2 us -> 12 us
  matrix products: 39.4 us -> 31.9 us
    reduce_scatter x3 -> x0, waiting for transfers between devices: 296 us -> none  [the longest x1 268 us: per_device(): lax.psum_scatter(jnp.concatenate([column_product(normed_all, d_gate), col...]
    all_gather x6 -> x0, waiting for transfers between devices: 241 us -> none  [the longest x1 61.6 us: per_device(): lax.all_gather(gate_weight, 'fs', axis=0, tiled=True)]
    pallas_call x0 -> x2, Pallas kernels: none -> 188 us  [the longest x1 96.8 us: reduce(): pl.pallas_call(functools.partial(reduce_kernel, n, n_tp), out_shape=[jax....]
    psum x1 -> x0, blocking collectives: 40.6 us -> none  [per_device(): gain_sum_out = gain_sum + lax.psum(gain_part, ('fs', 'tp'))]
    dot_general x4 -> x3, matrix products: 20.6 us -> 12.2 us  [the longest x1 6.56 us: per_device(): both = jnp.dot(late_all, gu_all, preferred_element_type=jnp.float32)]
    unnamed x32 -> x48, local copies, waits for them, and re-layouts: 3.2 us -> 11.4 us
    dot_general x3 -> x2, matrix products: 5.07 us -> 11.7 us  [column_product(): lax.dot_general(left, right, (((0,), (0,)), ((), ())), preferred_element_...]
    dot_general x3 -> x2, matrix products: 13.8 us -> 8 us  [times_transposed(): lax.dot_general(left, right, (((1,), (1,)), ((), ())), preferred_element_...]
  transfers between devices with their start and end apart: 9 -> 0, of which waited for: 8 -> 0; matrix products, arithmetic and copies ran while one was open for 4% -> 0% of each run, Pallas kernels for 0% -> 0%
where the time goes in v1:
time: 250 us; the launch traced here: 249 us
  Pallas kernels  188 us (75%)
  matrix products  31.9 us (13%)
  other arithmetic  15.8 us (6%)
  local copies, waits for them, and re-layouts  12 us (5%)
    pallas_call x1, Pallas kernels, reduce(): pl.pallas_call(functools.partial(reduce_kernel, n, n_tp), out_shape=[jax....  96.8 us
    pallas_call x1, Pallas kernels, gather(): pl.pallas_call(functools.partial(gather_kernel, n, n_tp), out_shape=[jax....  91.7 us
    dot_general x2, matrix products, column_product(): lax.dot_general(left, right, (((0,), (0,)), ((), ())), preferred_element_...  11.7 us
    unnamed x48, local copies, waits for them, and re-layouts  11.4 us
    dot_general x2, matrix products, times_transposed(): lax.dot_general(left, right, (((1,), (1,)), ((), ())), preferred_element_...  8 us
    dot_general x1, matrix products, per_device(): both = jnp.dot(late_all, gu_all, preferred_element_type=jnp.float32)  6.56 us

profile of v1, /device:TPU:0, one launch (start us, length us, event | category | flops | bytes accessed | tf_op | source)
XLA Modules:
  0.0 249.1 jit_solution(8442681770485158110)
XLA Ops:
  0.6 1.3 fusion.1
  1.9 1.3 fusion.5
  3.2 0.7 convert_element_type.97
  3.9 1.2 copy.28
  5.1 1.2 copy.29
  6.3 1.1 pad_maximum_fusion.3.refs_0_
  7.4 0.9 copy.30.refs_1_
  8.3 0.3 copy.34
  8.6 1.2 copy.35
  9.8 1.4 copy.36
  11.2 1.3 fusion.7
  12.5 91.7 %shard_map.154 = (bf16[2048,1408]{1,0:T(8,128)(2,1)}, bf16[2048,704]{1,0:T(8,128)(2,1)}, bf16[512,2048]{1,0:T(8,128)(2,1)}, bf16[512,2048]{1,0:T(8,128)(2,1)}, bf16[512,2048]{1,0:T(8,128)(2,1)}) custom-call(bf16[256,1408]{1,0:T(8,128)(2,1)} %pad_maximum_fusion.3.refs_0_, bf16[256,704]{1,0:T(8,128)(2,1)} %copy.30.refs_1_, ...), custom_call_target="tpu_custom_call" | custom-call | tf_op jit(solution)/shard_map/pallas_call | solution.py:151
  104.2 6.6 %fusion.21 = f32[512,1408]{1,0:T(8,128)S(1)} fusion(bf16[512,2048]{1,0:T(8,128)(2,1)} %get-tuple-element.16, bf16[2048,1408]{1,0:T(8,128)(2,1)} %get-tuple-element.17), kind=kOutput, calls=%fused_computation.53 | convolution fusion | flops 2952790016 | bytes 10747904 | tf_op jit(solution)/shard_map/dot_general | solution.py:391
  110.8 3.3 %convolution_convert_fusion.1.refs_2_ = bf16[512,2048]{1,0:T(8,128)(2,1)} fusion(bf16[2048,704]{1,0:T(8,128)(2,1)S(1)} %copy-done.14, f32[512,1408]{1,0:T(8,128)S(1)} %fusion.21), kind=kOutput, calls=%fused_computation.3 | convolution fusion | flops 1479606272 | bytes 8388608 | tf_op jit(solution)/shard_map/dot_general | solution.py:341
  114.1 0.7 copy-done.15
  114.8 3.4 %fusion.22 = f32[512,1408]{1,0:T(8,128)S(1)} fusion(bf16[512,2048]{1,0:T(8,128)(2,1)S(1)} %copy-done.15, bf16[2048,1408]{1,0:T(8,128)(2,1)S(1)} %copy-done.13), kind=kOutput, calls=%fused_computation.54 | convolution fusion | flops 2952790016 | bytes 10747904 | tf_op jit(solution)/shard_map/dot_general | solution.py:377
  118.2 2.2 multiply_convert_fusion.3
  120.5 3.7 %multiply_convert_fusion.refs_1_ = bf16[2048,704]{1,0:T(8,128)(2,1)} fusion(bf16[512,2048]{1,0:T(8,128)(2,1)S(1)} %copy-done.16, f32[512,1408]{1,0:T(8,128)S(1)} %fusion.22), kind=kOutput, calls=%fused_computation.1 | convolution fusion | flops 1481441280 | bytes 8126464 | tf_op jit(solution)/shard_map/dot_general | solution.py:347
  124.2 4.7 %multiply_reduce_fusion = (f32[2048]{0:T(1024)S(1)}, bf16[512,2048]{1,0:T(8,128)(2,1)}) fusion(bf16[512,2048]{1,0:T(8,128)(2,1)S(1)} %copy-done.15, bf16[2048,1408]{1,0:T(8,128)(2,1)S(1)} %copy-done.13, bf16[512,704]{1,0:T(8,128)(2,1)S(1)} %get-tuple-element.39, bf16[512,704]{1,0:T(8,128)(2,1)S(1)} %get-tuple-element.38), kind=kOutput, calls=%fused_computation.2 | convolution fusion | flops 2960914432 | bytes 11411456 | tf_op jit(solution)/shard_map/dot_general | solution.py:341
  128.9 0.6 reshape.57.refs_4_
  129.5 8.0 %convolution_convert_fusion.refs_0_ = bf16[2048,1408]{1,0:T(8,128)(2,1)} fusion(bf16[512,2048]{1,0:T(8,128)(2,1)} %get-tuple-element.19, bf16[512,704]{1,0:T(8,128)(2,1)} %copy-done.18, bf16[512,704]{1,0:T(8,128)(2,1)} %copy-done.17), kind=kOutput, calls=%fused_computation | convolution fusion | flops 2958557184 | bytes 9306112 | tf_op jit(solution)/shard_map/dot_general | solution.py:347
  137.5 96.8 %shard_map.155 = (f32[256,1408]{1,0:T(8,128)}, f32[256,704]{1,0:T(8,128)}, bf16[3,128,2048]{2,1,0:T(8,128)(2,1)}, bf16[3,128,2048]{2,1,0:T(8,128)(2,1)}, f32[8,256]{1,0:T(8,128)}) custom-call(bf16[2048,1408]{1,0:T(8,128)(2,1)} %convolution_convert_fusion.refs_0_, bf16[2048,704]{1,0:T(8,128)(2,1)} %multiply_convert_fusion.refs_1_, ...), custom_call_target="tpu_custom_call" | custom-call | tf_op jit(solution)/shard_map/pallas_call | solution.py:303
  234.3 1.2 add.85
  235.5 1.1 copy.39
  236.6 2.9 %fusion.4 = bf16[128,2048]{1,0:T(8,128)(2,1)} fusion(bf16[128,2048]{1,0:T(8,128)(2,1)S(1)} %copy-done.2, bf16[3,128,2048]{2,1,0:T(8,128)(2,1)} %get-tuple-element.21, bf16[512,2048]{1,0:T(8,128)(2,1)} %convolution_convert_fusion.1.refs_2_, s32[]{:T(128)S(6)} %select_n.4), kind=kLoop, calls=%fused_computation.23 | loop fusion | flops 2883584 | bytes 3145732 | tf_op jit(solution)/shard_map/convert_element_type | solution.py:405
  239.5 1.5 slice_add_fusion
  241.0 2.3 copy.38
  243.3 1.5 fusion.11
  244.9 0.0 copy-start.11
  244.9 2.5 fusion.10
  247.4 0.6 add.86
  248.0 1.1 copy.37
  (40 shorter events, 0.1 us)
Async XLA Ops:
  0.6 6.8 %copy-start.9 = (bf16[256,704]{0,1:T(8,128)(2,1)S(1)}, bf16[256,704]{0,1:T(8,128)(2,1)}, u32[]{:S(2)}) copy-start(bf16[256,704]{0,1:T(8,128)(2,1)} %param.15) | copy-start | bytes 1081348
  1.9 6.4 %copy-start.7 = (f32[256,704]{0,1:T(8,128)S(1)}, f32[256,704]{0,1:T(8,128)}, u32[]{:S(2)}) copy-start(f32[256,704]{0,1:T(8,128)} %param.18) | copy-start | bytes 2162692
  5.1 3.5 %copy-start.8 = (f32[256,704]{0,1:T(8,128)S(1)}, f32[256,704]{0,1:T(8,128)}, u32[]{:S(2)}) copy-start(f32[256,704]{0,1:T(8,128)} %param.19) | copy-start | bytes 2162692
  8.3 2.8 %copy-start = (bf16[128,2048]{1,0:T(8,128)(2,1)S(1)}, bf16[128,2048]{1,0:T(8,128)(2,1)}, u32[]{:S(2)}) copy-start(bf16[128,2048]{1,0:T(8,128)(2,1)} %param.16) | copy-start | bytes 1572868
  8.3 2.9 %copy-start.2 = (bf16[128,2048]{1,0:T(8,128)(2,1)S(1)}, bf16[128,2048]{1,0:T(8,128)(2,1)}, u32[]{:S(2)}) copy-start(bf16[128,2048]{1,0:T(8,128)(2,1)} %param.11) | copy-start | bytes 1572868
  104.2 6.6 %copy-start.14 = (bf16[2048,704]{1,0:T(8,128)(2,1)S(1)}, bf16[2048,704]{1,0:T(8,128)(2,1)}, u32[]{:S(2)}) copy-start(bf16[2048,704]{1,0:T(8,128)(2,1)} %get-tuple-element.18) | copy-start | bytes 8650756
  110.7 3.3 %copy-start.13 = (bf16[2048,1408]{1,0:T(8,128)(2,1)S(1)}, bf16[2048,1408]{1,0:T(8,128)(2,1)}, u32[]{:S(2)}) copy-start(bf16[2048,1408]{1,0:T(8,128)(2,1)} %get-tuple-element.17) | copy-start | bytes 17301508
  110.8 4.0 %copy-start.15 = (bf16[512,2048]{1,0:T(8,128)(2,1)S(1)}, bf16[512,2048]{1,0:T(8,128)(2,1)}, u32[]{:S(2)}) copy-start(bf16[512,2048]{1,0:T(8,128)(2,1)} %get-tuple-element.19) | copy-start | bytes 6291460
  114.8 3.4 %copy-start.16 = (bf16[512,2048]{1,0:T(8,128)(2,1)S(1)}, bf16[512,2048]{1,0:T(8,128)(2,1)}, u32[]{:S(2)}) copy-start(bf16[512,2048]{1,0:T(8,128)(2,1)} %get-tuple-element.20) | copy-start | bytes 6291460
  120.4 3.8 %copy-start.17 = (bf16[512,704]{1,0:T(8,128)(2,1)}, bf16[512,704]{1,0:T(8,128)(2,1)S(1)}, u32[]{:S(2)}) copy-start(bf16[512,704]{1,0:T(8,128)(2,1)S(1)} %get-tuple-element.38) | copy-start | bytes 2162692
  120.5 3.8 %copy-start.18 = (bf16[512,704]{1,0:T(8,128)(2,1)}, bf16[512,704]{1,0:T(8,128)(2,1)S(1)}, u32[]{:S(2)}) copy-start(bf16[512,704]{1,0:T(8,128)(2,1)S(1)} %get-tuple-element.39) | copy-start | bytes 2162692
  124.2 4.7 %copy-start.10 = (bf16[2048]{0:T(1024)(128)(2,1)S(1)}, bf16[2048]{0:T(1024)(128)(2,1)}, u32[]{:S(2)}) copy-start(bf16[2048]{0:T(1024)(128)(2,1)} %param.12) | copy-start | bytes 12292
  236.6 2.9 %copy-start.3 = (f32[256,704]{1,0:T(8,128)S(1)}, f32[256,704]{1,0:T(8,128)}, u32[]{:S(2)}) copy-start(f32[256,704]{1,0:T(8,128)} %copy.35) | copy-start | bytes 2162692
  236.6 2.9 %copy-start.6 = (f32[256,1408]{1,0:T(8,128)S(1)}, f32[256,1408]{1,0:T(8,128)}, u32[]{:S(2)}) copy-start(f32[256,1408]{1,0:T(8,128)} %get-tuple-element.23) | copy-start | bytes 4325380
  239.5 3.8 %copy-start.1 = (bf16[3,128,2048]{2,1,0:T(8,128)(2,1)S(1)}, bf16[3,128,2048]{2,1,0:T(8,128)(2,1)}, u32[]{:S(2)}) copy-start(bf16[3,128,2048]{2,1,0:T(8,128)(2,1)} %get-tuple-element.22) | copy-start | bytes 4718596
  241.0 3.9 %copy-start.5 = (bf16[128,2048]{1,0:T(8,128)(2,1)S(1)}, bf16[128,2048]{1,0:T(8,128)(2,1)}, u32[]{:S(2)}) copy-start(bf16[128,2048]{1,0:T(8,128)(2,1)} %refs_4_.1) | copy-start | bytes 1572868
  244.9 2.5 %copy-start.12 = (f32[8,256]{1,0:T(8,128)S(1)}, f32[8,256]{1,0:T(8,128)}, u32[]{:S(2)}) copy-start(f32[8,256]{1,0:T(8,128)} %get-tuple-element.25) | copy-start | bytes 24580
  244.9 2.5 %copy-start.11 = (f32[2048]{0:T(1024)S(1)}, f32[2048]{0:T(1024)}, u32[]{:S(2)}) copy-start(f32[2048]{0:T(1024)} %param.21) | copy-start | bytes 24580
  244.9 3.1 %copy-start.4 = (f32[256,704]{1,0:T(8,128)S(1)}, f32[256,704]{1,0:T(8,128)}, u32[]{:S(2)}) copy-start(f32[256,704]{1,0:T(8,128)} %get-tuple-element.41) | copy-start | bytes 2162692

commit v2 on v1

--- a/solution.py
+++ b/solution.py
@@ -44,15 +44,32 @@
 
 
 def gather_kernel(n, n_tp, *refs):
-    gu_ref, dn_ref, late_ref, early_ref, cot_ref = refs[:5]
-    gu_all, dn_all, late_all, early_all, cot_all = refs[5:10]
-    send_sem, recv_sem, tp_send, tp_recv, own_sem = refs[10:]
+    gate_in, up_in, dn_ref, late_in, early_in, cot_ref, gain_ref = refs[:7]
+    gu_all, dn_all, late_all, early_all, cot_all = refs[7:12]
+    gate_buf, up_buf, gu_ref, dn_buf, late_buf, early_buf, cot_buf, late_ref, early_ref = refs[12:21]
+    send_sem, recv_sem, tp_send, tp_recv, own_sem, in_sem = refs[21:]
+    width = gate_in.shape[1]
+    loads = [
+        pltpu.make_async_copy(source, target, in_sem.at[k])
+        for k, (source, target) in enumerate(
+            (
+                (gate_in, gate_buf),
+                (up_in, up_buf),
+                (early_in, early_buf),
+                (late_in, late_buf),
+                (dn_ref, dn_buf),
+                (cot_ref, cot_buf),
+            )
+        )
+    ]
+    for copy in loads:
+        copy.start()
     me_fs, me_tp = lax.axis_index("fs"), lax.axis_index("tp")
     place, right, left = neighbours(n)
     greet(n_tp, right, left)
-    rows = gu_ref.shape[0]
+    rows = gate_in.shape[0]
     half = rows // 2
-    tokens = late_ref.shape[0]
+    tokens = late_in.shape[0]
     pairs = ((gu_ref, gu_all), (dn_ref, dn_all))
 
     def window(owner, way):
@@ -77,35 +94,60 @@
             device_id_type=MESH,
         )
 
-    for c in range(2):
-        for way in range(2):
-            piece(0, c, way, True).start()
-
+    mine = pl.ds(pl.multiple_of(me_tp * tokens, tokens), tokens)
     token_pairs = ((early_ref, early_all), (cot_ref, cot_all), (late_ref, late_all))
-    token_copies = []
-    for a, (block, whole) in enumerate(token_pairs):
+
+    def spread(a):
+        block, whole = token_pairs[a]
+        copies = []
         for away in range(1, n_tp):
             peer = lax.rem(me_tp + away, n_tp)
             copy = pltpu.make_async_remote_copy(
                 src_ref=block,
-                dst_ref=whole.at[pl.ds(pl.multiple_of(me_tp * tokens, tokens), tokens)],
+                dst_ref=whole.at[mine],
                 send_sem=tp_send.at[a, away - 1],
                 recv_sem=tp_recv.at[a, away - 1],
                 device_id=(me_fs, peer),
                 device_id_type=MESH,
             )
             copy.start()
-            token_copies.append(copy)
+            copies.append(copy)
+        return copies
+
+    def norm(source, target):
+        def part(k, carry):
+            some = pl.ds(pl.multiple_of(k * 16, 16), 16)
+            values = source[some, :].astype(jnp.float32)
+            scale = lax.rsqrt(jnp.mean(values * values, axis=-1, keepdims=True) + epsilon)
+            target[some, :] = (values * scale * gain_ref[...]).astype(jnp.bfloat16)
+            return carry
+
+        lax.fori_loop(0, tokens // 16, part, 0)
+
+    for way in range(2):
+        piece(0, 1, way, True).start()
+    token_copies = spread(1)
+    loads[0].wait()
+    loads[1].wait()
+    gu_ref[:, :width] = gate_buf[...]
+    gu_ref[:, width:] = up_buf[...]
+    for way in range(2):
+        piece(0, 0, way, True).start()
+    loads[2].wait()
+    norm(early_buf, early_ref)
+    token_copies += spread(0)
+    loads[3].wait()
+    norm(late_buf, late_ref)
+    token_copies += spread(2)
+    loads[4].wait()
+    loads[5].wait()
     own = []
-    for a, (block, whole) in enumerate(token_pairs):
+    sources = (early_ref, cot_buf, late_ref)
+    for a in range(3):
         own.append(
-            pltpu.make_async_copy(
-                block,
-                whole.at[pl.ds(pl.multiple_of(me_tp * tokens, tokens), tokens)],
-                own_sem.at[a],
-            )
-        )
-    for c, (block, whole) in enumerate(pairs):
+            pltpu.make_async_copy(sources[a], token_pairs[a][1].at[mine], own_sem.at[a])
+        )
+    for c, (block, whole) in enumerate(((gu_ref, gu_all), (dn_buf, dn_all))):
         own.append(
             pltpu.make_async_copy(
                 block,
@@ -117,20 +159,20 @@
         copy.start()
 
     def body(step, carry):
-        for c in range(2):
+        for c in (1, 0):
             for way in range(2):
                 piece(step - 1, c, way, False).wait_recv()
                 piece(step, c, way, False).start()
         return carry
 
     lax.fori_loop(1, n - 1, body, 0)
-    for c in range(2):
+    for c in (1, 0):
         for way in range(2):
             piece(n - 2, c, way, False).wait_recv()
             piece(0, c, way, True).wait_send()
 
     def drain(step, carry):
-        for c in range(2):
+        for c in (1, 0):
             for way in range(2):
                 piece(step, c, way, False).wait_send()
         return carry
@@ -142,8 +184,8 @@
         copy.wait()
 
 
-def gather(n, n_tp, gu, dn, late, early, cot):
-    rows, width2 = gu.shape
+def gather(n, n_tp, gate, up, dn, late, early, cot, gain):
+    rows, width = gate.shape
     tokens, depth = late.shape
     vmem = pl.BlockSpec(memory_space=pltpu.VMEM)
     hbm = pl.BlockSpec(memory_space=pl.ANY)
@@ -151,36 +193,66 @@
     return pl.pallas_call(
         functools.partial(gather_kernel, n, n_tp),
         out_shape=[
-            jax.ShapeDtypeStruct((n * rows, width2), bf16),
-            jax.ShapeDtypeStruct((n * rows, dn.shape[1]), bf16),
+            jax.ShapeDtypeStruct((n * rows, 2 * width), bf16),
+            jax.ShapeDtypeStruct((n * rows, width), bf16),
         ]
         + [jax.ShapeDtypeStruct((n_tp * tokens, depth), bf16)] * 3,
-        in_specs=[vmem] * 5,
+        in_specs=[hbm] * 6 + [vmem],
         out_specs=[hbm] * 5,
         scratch_shapes=[
+            pltpu.VMEM((rows, width), bf16),
+            pltpu.VMEM((rows, width), bf16),
+            pltpu.VMEM((rows, 2 * width), bf16),
+            pltpu.VMEM((rows, width), bf16),
+        ]
+        + [pltpu.VMEM((tokens, depth), bf16)] * 5
+        + [
             pltpu.SemaphoreType.DMA((n - 1, 2, 2)),
             pltpu.SemaphoreType.DMA((n - 1, 2, 2)),
             pltpu.SemaphoreType.DMA((3, n_tp - 1)),
             pltpu.SemaphoreType.DMA((3, n_tp - 1)),
             pltpu.SemaphoreType.DMA((5,)),
+            pltpu.SemaphoreType.DMA((6,)),
         ],
         compiler_params=pltpu.CompilerParams(
             collective_id=0, has_side_effects=True, vmem_limit_bytes=VMEM_LIMIT
         ),
-    )(gu, dn, late, early, cot)
+    )(gate, up, dn, late, early, cot, gain)
 
 
 def reduce_kernel(n, n_tp, *refs):
-    gu_ref, dn_ref, mix_ref, dnorm_ref, gain_ref = refs[:5]
-    gu_out, dn_out, mix_out, dnorm_out, gain_out = refs[5:10]
-    (gu_slots, dn_slots, gain_slots, gain_tp) = refs[10:14]
-    send_sem, recv_sem, gain_send, gain_recv, tp_send, tp_recv, last_send, last_recv = refs[14:]
+    gu_ref, dn_ref, both_ref, gain_ref, gu_in, dn_in, late_in, early_in = refs[:8]
+    gu_out, dn_out, mix_out, dnorm_out, gain_out = refs[8:13]
+    gu_slots, dn_slots, gain_slots, gain_tp = refs[13:17]
+    gu_all, dn_all, late_all, early_all, mix_ref, dnorm_ref, gain_sum = refs[17:24]
+    send_sem, recv_sem, gain_send, gain_recv, tp_send, tp_recv, last_send, last_recv = refs[24:32]
+    in_sem, own_sem = refs[32:]
+    loads = [
+        pltpu.make_async_copy(source, target, in_sem.at[k])
+        for k, (source, target) in enumerate(
+            ((gu_in, gu_all), (early_in, early_all), (late_in, late_all), (dn_in, dn_all))
+        )
+    ]
+    for copy in loads:
+        copy.start()
     me_fs, me_tp = lax.axis_index("fs"), lax.axis_index("tp")
     place, right, left = neighbours(n)
-    greet(n_tp, right, left)
+    barrier = pltpu.get_barrier_semaphore()
+
+    def greet_fs(away, carry):
+        target = lax.rem(me_fs + away, n)
+        pl.semaphore_signal(barrier, inc=1, device_id=(target, me_tp), device_id_type=MESH)
+        return carry
+
+    lax.fori_loop(1, n, greet_fs, 0)
+    for away in range(1, n_tp):
+        peer = lax.rem(me_tp + away, n_tp)
+        pl.semaphore_signal(barrier, inc=1, device_id=(me_fs, peer), device_id_type=MESH)
+    pl.semaphore_wait(barrier, n - 1 + n_tp - 1)
+    width = dn_all.shape[1]
     rows = gu_ref.shape[0] // n
     half = rows // 2
-    tokens = mix_ref.shape[0] // n_tp
+    tokens = late_all.shape[0] // n_tp
     sets = ((gu_ref, gu_slots, gu_out), (dn_ref, dn_slots, dn_out))
 
     def local(step, way):
@@ -202,35 +274,67 @@
             device_id_type=MESH,
         )
 
-    def gain_piece(step):
+    def gain_piece(away):
         return pltpu.make_async_remote_copy(
-            src_ref=gain_slots.at[ring_index(lax.rem(place - step + n, n), n)],
-            dst_ref=gain_slots.at[ring_index(lax.rem(place - step + n, n), n)],
-            send_sem=gain_send.at[step],
-            recv_sem=gain_recv.at[step],
-            device_id=(right, me_tp),
+            src_ref=gain_slots.at[me_fs],
+            dst_ref=gain_slots.at[me_fs],
+            send_sem=gain_send.at[away - 1],
+            recv_sem=gain_recv.at[away - 1],
+            device_id=(lax.rem(me_fs + away, n), me_tp),
             device_id_type=MESH,
         )
 
-    gain_slots[me_fs] = gain_ref[...]
+    results = ((dnorm_ref, dnorm_out), (mix_ref, mix_out))
+
+    def share(a, away):
+        source, target = results[a]
+        return pltpu.make_async_remote_copy(
+            src_ref=source.at[away - 1],
+            dst_ref=target.at[away - 1],
+            send_sem=tp_send.at[a, away - 1],
+            recv_sem=tp_recv.at[a, away - 1],
+            device_id=(me_fs, lax.rem(me_tp + away, n_tp)),
+            device_id_type=MESH,
+        )
+
+    def keep(a):
+        source, target = results[a]
+        return pltpu.make_async_copy(source.at[n_tp - 1], target.at[n_tp - 1], own_sem.at[a])
+
+    def block_of(away):
+        return pl.ds(pl.multiple_of(lax.rem(me_tp + away, n_tp) * tokens, tokens), tokens)
+
+    def grad_block(away):
+        some = block_of(away)
+        part = lax.dot_general(
+            both_ref[some, :],
+            gu_all[...],
+            (((1,), (1,)), ((), ())),
+            preferred_element_type=jnp.float32,
+        ).astype(jnp.bfloat16)
+        dnorm_ref[away - 1] = part
+        gain_sum[...] += jnp.sum(
+            part.astype(jnp.float32) * early_all[some, :].astype(jnp.float32),
+            axis=0,
+            keepdims=True,
+        )
+
+    def late_block(away):
+        both = jnp.dot(
+            late_all[block_of(away), :], gu_all[...], preferred_element_type=jnp.float32
+        )
+        gate = both[:, :width]
+        hidden = (gate / (1.0 + jnp.exp(-gate)) * both[:, width:]).astype(jnp.bfloat16)
+        mix_ref[away - 1] = lax.dot_general(
+            hidden, dn_all[...], (((1,), (1,)), ((), ())), preferred_element_type=jnp.float32
+        ).astype(jnp.bfloat16)
+
     for c in range(2):
         for way in range(2):
             piece(0, c, way, True).start()
-    tp_copies = []
-    for a, (source, target) in enumerate(((dnorm_ref, dnorm_out), (mix_ref, mix_out))):
-        for away in range(1, n_tp):
-            peer = lax.rem(me_tp + away, n_tp)
-            copy = pltpu.make_async_remote_copy(
-                src_ref=source.at[pl.ds(pl.multiple_of(peer * tokens, tokens), tokens)],
-                dst_ref=target.at[away - 1],
-                send_sem=tp_send.at[a, away - 1],
-                recv_sem=tp_recv.at[a, away - 1],
-                device_id=(me_fs, peer),
-                device_id_type=MESH,
-            )
-            copy.start()
-            tp_copies.append(copy)
-    gain_piece(0).start()
+    gain_sum[...] = jnp.zeros_like(gain_sum)
+    for copy in loads:
+        copy.wait()
 
     def body(step, carry):
         for c in range(2):
@@ -242,16 +346,41 @@
                     + partial[local(step, way), :].astype(jnp.float32)
                 ).astype(jnp.bfloat16)
                 piece(step, c, way, False).start()
-        gain_piece(step - 1).wait_recv()
-        gain_piece(step).start()
+
+            @pl.when(step <= n_tp)
+            def _():
+                (grad_block, late_block)[c](step)
+
+            @pl.when(step < n_tp)
+            def _():
+                share(c, step).start()
+
+            @pl.when(step == n_tp)
+            def _():
+                keep(c).start()
+
+        @pl.when(step == n_tp)
+        def _():
+            gain_slots[me_fs] = gain_sum[...] / gain_ref[...]
+
+            def send(away, inner):
+                gain_piece(away).start()
+                return inner
+
+            lax.fori_loop(1, n, send, 0)
+
         return carry
 
     lax.fori_loop(1, n - 1, body, 0)
-    gain_piece(n - 2).wait_recv()
-    total = gain_slots[0]
-    for k in range(1, n):
-        total = total + gain_slots[k]
-    gain_tp[me_tp] = total
+
+    def settle(away, inner):
+        gain_piece(away).wait()
+        return inner
+
+    lax.fori_loop(1, n, settle, 0)
+    gain_tp[me_tp] = lax.fori_loop(
+        1, n, lambda k, total: total + gain_slots[k], gain_slots[0]
+    )
     last = []
     for away in range(1, n_tp):
         peer = lax.rem(me_tp + away, n_tp)
@@ -284,19 +413,20 @@
         for c in range(2):
             for way in range(2):
                 piece(step, c, way, False).wait_send()
-        gain_piece(step).wait_send()
         return carry
 
-    gain_piece(0).wait_send()
     lax.fori_loop(1, n - 1, drain, 0)
-    for copy in tp_copies:
-        copy.wait()
-
-
-def reduce(n, n_tp, gu, dn, mix, dnorm, gain):
+    for a in range(2):
+        keep(a).wait()
+        for away in range(1, n_tp):
+            share(a, away).wait()
+
+
+def reduce(n, n_tp, gu, dn, both, gain, gu_all, dn_all, late_all, early_all):
     rows = gu.shape[0] // n
     half = rows // 2
-    tokens = mix.shape[0] // n_tp
+    depth = late_all.shape[1]
+    tokens = late_all.shape[0] // n_tp
     vmem = pl.BlockSpec(memory_space=pltpu.VMEM)
     hbm = pl.BlockSpec(memory_space=pl.ANY)
     f32, bf16 = jnp.float32, jnp.bfloat16
@@ -305,17 +435,24 @@
         out_shape=[
             jax.ShapeDtypeStruct((rows, gu.shape[1]), f32),
             jax.ShapeDtypeStruct((rows, dn.shape[1]), f32),
-            jax.ShapeDtypeStruct((n_tp - 1, tokens, mix.shape[1]), bf16),
-            jax.ShapeDtypeStruct((n_tp - 1, tokens, mix.shape[1]), bf16),
+            jax.ShapeDtypeStruct((n_tp, tokens, depth), bf16),
+            jax.ShapeDtypeStruct((n_tp, tokens, depth), bf16),
             jax.ShapeDtypeStruct(gain.shape, f32),
         ],
-        in_specs=[vmem, vmem, hbm, hbm, vmem],
+        in_specs=[vmem] * 4 + [hbm] * 4,
         out_specs=[vmem, vmem, hbm, hbm, vmem],
         scratch_shapes=[
             pltpu.VMEM((2, n - 1, half, gu.shape[1]), bf16),
             pltpu.VMEM((2, n - 1, half, dn.shape[1]), bf16),
             pltpu.VMEM((n,) + gain.shape, f32),
             pltpu.VMEM((n_tp,) + gain.shape, f32),
+            pltpu.VMEM(gu_all.shape, bf16),
+            pltpu.VMEM(dn_all.shape, bf16),
+            pltpu.VMEM(late_all.shape, bf16),
+            pltpu.VMEM(early_all.shape, bf16),
+            pltpu.VMEM((n_tp, tokens, depth), bf16),
+            pltpu.VMEM((n_tp, tokens, depth), bf16),
+            pltpu.VMEM(gain.shape, f32),
             pltpu.SemaphoreType.DMA((n - 1, 2, 2)),
             pltpu.SemaphoreType.DMA((n - 1, 2, 2)),
             pltpu.SemaphoreType.DMA((n - 1,)),
@@ -324,23 +461,13 @@
             pltpu.SemaphoreType.DMA((2, n_tp - 1)),
             pltpu.SemaphoreType.DMA((n_tp - 1,)),
             pltpu.SemaphoreType.DMA((n_tp - 1,)),
+            pltpu.SemaphoreType.DMA((4,)),
+            pltpu.SemaphoreType.DMA((2,)),
         ],
         compiler_params=pltpu.CompilerParams(
             collective_id=1, has_side_effects=True, vmem_limit_bytes=VMEM_LIMIT
         ),
-    )(gu, dn, mix, dnorm, gain)
-
-
-def normalize(source, gain_f):
-    values = source.astype(jnp.float32)
-    scale = lax.rsqrt(jnp.mean(values * values, axis=-1, keepdims=True) + epsilon)
-    return ((values * scale * gain_f).astype(jnp.bfloat16), scale, values)
-
-
-def times_transposed(left, right):
-    return lax.dot_general(
-        left, right, (((1,), (1,)), ((), ())), preferred_element_type=jnp.float32
-    )
+    )(gu, dn, both, gain, gu_all, dn_all, late_all, early_all)
 
 
 def column_product(left, right):
@@ -367,12 +494,9 @@
     gain_f = norm_gain.astype(jnp.float32)
     width = gate_weight.shape[1]
     depth = late_input.shape[1]
-    tokens = late_input.shape[0]
-    normed, _, values = normalize(late_input, gain_f)
-    normed_e, scale_e, values_e = normalize(early_input, gain_f)
-    gu = jnp.concatenate([gate_weight, up_weight], axis=1)
+    gain_row = gain_f.reshape(1, depth)
     gu_all, down_all, late_all, early_all, cot_all = gather(
-        n, n_tp, gu, down_weight, normed, normed_e, cotangent
+        n, n_tp, gate_weight, up_weight, down_weight, late_input, early_input, cotangent, gain_row
     )
     both_e = jnp.dot(early_all, gu_all, preferred_element_type=jnp.float32)
     gate_e, upper_e = both_e[:, :width], both_e[:, width:]
@@ -382,28 +506,23 @@
     d_gate = (d_hidden * upper_e * sigma_e * (1.0 + gate_e * (1.0 - sigma_e))).astype(jnp.bfloat16)
     d_up = (d_hidden * gate_e * sigma_e).astype(jnp.bfloat16)
     d_both = jnp.concatenate([d_gate, d_up], axis=1)
-    d_part = times_transposed(d_both, gu_all).astype(jnp.bfloat16)
-    gain_part = (
-        jnp.sum(d_part.astype(jnp.float32) * early_all.astype(jnp.float32), axis=0) / gain_f
-    )
     gu_part = column_product(early_all, d_both).astype(jnp.bfloat16)
     down_part = (0.5 * column_product(cot_all, hidden_e)).astype(jnp.bfloat16)
-    both = jnp.dot(late_all, gu_all, preferred_element_type=jnp.float32)
-    hidden = (jax.nn.silu(both[:, :width]) * both[:, width:]).astype(jnp.bfloat16)
-    mix_part = times_transposed(hidden, down_all).astype(jnp.bfloat16)
     gu_grad, down_grad, mix_got, d_got, gain_total = reduce(
-        n, n_tp, gu_part, down_part, mix_part, d_part, gain_part.reshape(8, depth // 8)
+        n, n_tp, gu_part, down_part, d_both, gain_row, gu_all, down_all, late_all, early_all
     )
-    start = lax.axis_index("tp") * tokens
-
-    def gathered(part, got):
-        total = lax.dynamic_slice_in_dim(part, start, tokens, 0).astype(jnp.float32)
-        for k in range(n_tp - 1):
+
+    def gathered(got):
+        total = got[0].astype(jnp.float32)
+        for k in range(1, n_tp):
             total = total + got[k].astype(jnp.float32)
         return total
 
-    late_out = (values + 0.5 * gathered(mix_part, mix_got)).astype(jnp.bfloat16)
-    scaled_grad = gathered(d_part, d_got) * gain_f
+    values = late_input.astype(jnp.float32)
+    values_e = early_input.astype(jnp.float32)
+    scale_e = lax.rsqrt(jnp.mean(values_e * values_e, axis=-1, keepdims=True) + epsilon)
+    late_out = (values + 0.5 * gathered(mix_got)).astype(jnp.bfloat16)
+    scaled_grad = gathered(d_got) * gain_f
     early_grad = (
         cotangent.astype(jnp.float32)
         + scale_e * scaled_grad

time: 250 us -> 228 us (0.912)
  matrix products: 31.9 us -> 17.8 us
  other arithmetic: 15.8 us -> 10.4 us
    dot_general x3 -> x0, matrix products: 14.6 us -> none  [the longest x2 8 us: times_transposed(): lax.dot_general(left, right, (((1,), (1,)), ((), ())), preferred_element_...]
    convert_element_type x2 -> x0, other arithmetic: 4.17 us -> none  [the longest x1 2.9 us: per_device(): late_out = (values + 0.5 * gathered(mix_part, mix_got)).astype(jnp.bfloat16)]
    dot_general x1, matrix products: 3.4 us -> 6.56 us  [per_device(): both_e = jnp.dot(early_all, gu_all, preferred_element_type=jnp.float32)]
    dot_general x2, matrix products: 11.7 us -> 9.01 us  [column_product(): lax.dot_general(left, right, (((0,), (0,)), ((), ())), preferred_element_...]
    unnamed x48 -> x35, local copies, waits for them, and re-layouts: 11.4 us -> 11.9 us
where the time goes in v2:
time: 228 us
  Pallas kernels  187 us (82%)
  matrix products  17.8 us (8%)
  local copies, waits for them, and re-layouts  11.9 us (5%)
  other arithmetic  10.4 us (5%)
    pallas_call x1, Pallas kernels, reduce(): pl.pallas_call(functools.partial(reduce_kernel, n, n_tp), out_shape=[jax....  96 us
    pallas_call x1, Pallas kernels, gather(): pl.pallas_call(functools.partial(gather_kernel, n, n_tp), out_shape=[jax....  91 us
    unnamed x35, local copies, waits for them, and re-layouts  11.9 us
    dot_general x2, matrix products, column_product(): lax.dot_general(left, right, (((0,), (0,)), ((), ())), preferred_element_...  9.01 us
    dot_general x1, matrix products, per_device(): both_e = jnp.dot(early_all, gu_all, preferred_element_type=jnp.float32)  6.56 us

profile of v2, /device:TPU:0, one launch (start us, length us, event | category | flops | bytes accessed | tf_op | source)
XLA Modules:
  0.0 227.9 jit_solution(10129465790178725751)
XLA Ops:
  0.6 1.3 convert_element_type.66
  1.9 1.9 copy.28.refs_0_
  3.8 1.9 copy.29.refs_1_
  5.7 1.9 copy.30.refs_2_
  7.6 91.0 %shard_map.154 = (bf16[2048,1408]{1,0:T(8,128)(2,1)}, bf16[2048,704]{1,0:T(8,128)(2,1)}, bf16[512,2048]{1,0:T(8,128)(2,1)}, bf16[512,2048]{1,0:T(8,128)(2,1)}, bf16[512,2048]{1,0:T(8,128)(2,1)}) custom-call(bf16[256,704]{1,0:T(8,128)(2,1)} %copy.28.refs_0_, bf16[256,704]{1,0:T(8,128)(2,1)} %copy.29.refs_1_, bf16[256,704]{1,0:T(8,128)(2,1)} %copy.30.refs_2_, ...), custom_call_target="tpu_custom_call" | custom-call | tf_op jit(solution)/shard_map/pallas_call | solution.py:193
  98.6 0.0 copy-start.3
  98.6 0.0 copy-start.12
  98.6 6.6 %fusion.8 = f32[512,1408]{1,0:T(8,128)S(1)} fusion(bf16[512,2048]{1,0:T(8,128)(2,1)} %get-tuple-element.16.refs_7_, bf16[2048,1408]{1,0:T(8,128)(2,1)} %get-tuple-element.19.refs_4_), kind=kOutput, calls=%fused_computation.26 | convolution fusion | flops 2952790016 | bytes 10747904 | tf_op jit(solution)/shard_map/dot_general | solution.py:501
  105.2 0.0 copy-done.3
  105.2 2.2 multiply_convert_fusion.3
  107.5 0.0 copy-start.5
  107.5 0.4 pad_maximum_fusion.refs_2_
  107.9 1.1 copy-done.5
  109.1 5.3 %convolution_convert_fusion.refs_0_ = bf16[2048,1408]{1,0:T(8,128)(2,1)} fusion(bf16[512,2048]{1,0:T(8,128)(2,1)S(1)} %copy-done.5, bf16[512,1408]{1,0:T(8,128)(2,1)S(1)} %pad_maximum_fusion.refs_2_), kind=kOutput, calls=%fused_computation | convolution fusion | flops 2955673600 | bytes 9306112 | tf_op jit(solution)/shard_map/dot_general | solution.py:474
  114.4 3.7 %multiply_convert_fusion.refs_1_ = bf16[2048,704]{1,0:T(8,128)(2,1)} fusion(bf16[512,2048]{1,0:T(8,128)(2,1)S(1)} %copy-done.12, f32[512,1408]{1,0:T(8,128)S(1)} %fusion.8), kind=kOutput, calls=%fused_computation.1 | convolution fusion | flops 1481441280 | bytes 8126464 | tf_op jit(solution)/shard_map/dot_general | solution.py:474
  118.1 96.0 %shard_map.155 = (f32[256,1408]{1,0:T(8,128)}, f32[256,704]{1,0:T(8,128)}, bf16[4,128,2048]{2,1,0:T(8,128)(2,1)}, bf16[4,128,2048]{2,1,0:T(8,128)(2,1)}, f32[1,2048]{1,0:T(1,128)}) custom-call(bf16[2048,1408]{1,0:T(8,128)(2,1)} %convolution_convert_fusion.refs_0_, bf16[2048,704]{1,0:T(8,128)(2,1)} %multiply_convert_fusion.refs_1_, ...), custom_call_target="tpu_custom_call" | custom-call | tf_op jit(solution)/shard_map/pallas_call | solution.py:433
  214.1 0.0 copy-done.6
  214.1 0.3 copy.34
  214.4 0.0 copy-done.7
  214.4 0.3 copy.35
  214.7 1.7 slice_add_fusion
  216.3 0.0 copy-start.8
  216.3 1.1 copy.37
  217.4 1.1 copy.38
  218.6 1.2 copy.36
  219.8 1.6 add.82
  221.4 1.1 copy.39
  222.5 3.4 %fusion = (f32[128]{0:T(128)S(1)}, f32[128]{0:T(128)S(1)}, bf16[128,2048]{1,0:T(8,128)(2,1)}) fusion(bf16[128,2048]{1,0:T(8,128)(2,1)S(1)} %copy-done.2, f32[2048]{0:T(1024)S(1)} %copy-done.9, bf16[4,128,2048]{2,1,0:T(8,128)(2,1)S(1)} %copy-done, bf16[4,128,2048]{2,1,0:T(8,128)(2,1)} %get-tuple-element.21, bf16[128,2048]{1,0:T(8,128)(2,1)} %refs_3_.1), kind=kLoop, calls=%fused_computation.11 | loop fusion | flops 6291200 | bytes 5776384 | tf_op jit(solution)/shard_map/reduce_sum | solution.py:523
  225.9 0.0 copy-done.4
  226.0 1.4 fusion.3
  227.3 0.0 copy-done.11
  227.3 0.6 add.83
  (18 shorter events, 0.0 us)
Async XLA Ops:
  98.6 6.6 %copy-start.3 = (bf16[2048,704]{1,0:T(8,128)(2,1)S(1)}, bf16[2048,704]{1,0:T(8,128)(2,1)}, u32[]{:S(2)}) copy-start(bf16[2048,704]{1,0:T(8,128)(2,1)} %get-tuple-element.18.refs_5_) | copy-start | bytes 8650756
  98.6 6.6 %copy-start.12 = (bf16[512,2048]{1,0:T(8,128)(2,1)S(1)}, bf16[512,2048]{1,0:T(8,128)(2,1)}, u32[]{:S(2)}) copy-start(bf16[512,2048]{1,0:T(8,128)(2,1)} %get-tuple-element.17) | copy-start | bytes 6291460
  107.5 1.6 copy-start.5
  109.0 5.3 %copy-start.1 = (bf16[512,1408]{1,0:T(8,128)(2,1)}, bf16[512,1408]{1,0:T(8,128)(2,1)S(1)}, u32[]{:S(2)}) copy-start(bf16[512,1408]{1,0:T(8,128)(2,1)S(1)} %pad_maximum_fusion.refs_2_) | copy-start | bytes 4325380
  118.1 96.0 %copy-start.6 = (f32[256,704]{0,1:T(8,128)S(1)}, f32[256,704]{0,1:T(8,128)}, u32[]{:S(2)}) copy-start(f32[256,704]{0,1:T(8,128)} %param.18) | copy-start | bytes 2162692
  118.1 96.3 %copy-start.7 = (f32[256,704]{0,1:T(8,128)S(1)}, f32[256,704]{0,1:T(8,128)}, u32[]{:S(2)}) copy-start(f32[256,704]{0,1:T(8,128)} %param.19) | copy-start | bytes 2162692
  216.3 2.2 copy-start.8
  219.8 2.7 %copy-start = (bf16[4,128,2048]{2,1,0:T(8,128)(2,1)S(1)}, bf16[4,128,2048]{2,1,0:T(8,128)(2,1)}, u32[]{:S(2)}) copy-start(bf16[4,128,2048]{2,1,0:T(8,128)(2,1)} %get-tuple-element.22) | copy-start | bytes 6291460
  219.8 2.7 %copy-start.2 = (bf16[128,2048]{1,0:T(8,128)(2,1)S(1)}, bf16[128,2048]{1,0:T(8,128)(2,1)}, u32[]{:S(2)}) copy-start(bf16[128,2048]{1,0:T(8,128)(2,1)} %refs_4_.1) | copy-start | bytes 1572868
  219.8 2.7 %copy-start.9 = (f32[2048]{0:T(1024)S(1)}, f32[2048]{0:T(1024)}, u32[]{:S(2)}) copy-start(f32[2048]{0:T(1024)} %convert_element_type.66) | copy-start | bytes 24580
  222.5 3.5 %copy-start.4 = (bf16[128,2048]{1,0:T(8,128)(2,1)S(1)}, bf16[128,2048]{1,0:T(8,128)(2,1)}, u32[]{:S(2)}) copy-start(bf16[128,2048]{1,0:T(8,128)(2,1)} %refs_5_.1) | copy-start | bytes 1572868
  225.9 1.4 copy-start.10
  225.9 1.4 copy-start.11

commit v3 on v2

--- a/solution.py
+++ b/solution.py
@@ -43,12 +43,13 @@
     pl.semaphore_wait(barrier, 2 + n_tp - 1)
 
 
-def gather_kernel(n, n_tp, *refs):
-    gate_in, up_in, dn_ref, late_in, early_in, cot_ref, gain_ref = refs[:7]
+def gather_kernel(n, n_tp, turned, *refs):
+    gate_in, up_in, dn_in, late_in, early_in, cot_ref, gain_ref = refs[:7]
     gu_all, dn_all, late_all, early_all, cot_all = refs[7:12]
-    gate_buf, up_buf, gu_ref, dn_buf, late_buf, early_buf, cot_buf, late_ref, early_ref = refs[12:21]
-    send_sem, recv_sem, tp_send, tp_recv, own_sem, in_sem = refs[21:]
-    width = gate_in.shape[1]
+    gate_buf, up_buf, gu_ref, dn_buf, dn_ref = refs[12:17]
+    late_buf, early_buf, cot_buf, late_ref, early_ref = refs[17:22]
+    send_sem, recv_sem, tp_send, tp_recv, own_sem, in_sem = refs[22:]
+    rows, width = dn_ref.shape
     loads = [
         pltpu.make_async_copy(source, target, in_sem.at[k])
         for k, (source, target) in enumerate(
@@ -57,7 +58,7 @@
                 (up_in, up_buf),
                 (early_in, early_buf),
                 (late_in, late_buf),
-                (dn_ref, dn_buf),
+                (dn_in, dn_buf),
                 (cot_ref, cot_buf),
             )
         )
@@ -67,7 +68,6 @@
     me_fs, me_tp = lax.axis_index("fs"), lax.axis_index("tp")
     place, right, left = neighbours(n)
     greet(n_tp, right, left)
-    rows = gate_in.shape[0]
     half = rows // 2
     tokens = late_in.shape[0]
     pairs = ((gu_ref, gu_all), (dn_ref, dn_all))
@@ -124,13 +124,18 @@
 
         lax.fori_loop(0, tokens // 16, part, 0)
 
+    def plain(buffer):
+        return buffer[...].T if turned else buffer[...]
+
+    loads[4].wait()
+    dn_ref[...] = plain(dn_buf)
     for way in range(2):
         piece(0, 1, way, True).start()
     token_copies = spread(1)
     loads[0].wait()
     loads[1].wait()
-    gu_ref[:, :width] = gate_buf[...]
-    gu_ref[:, width:] = up_buf[...]
+    gu_ref[:, :width] = plain(gate_buf)
+    gu_ref[:, width:] = plain(up_buf)
     for way in range(2):
         piece(0, 0, way, True).start()
     loads[2].wait()
@@ -139,7 +144,6 @@
     loads[3].wait()
     norm(late_buf, late_ref)
     token_copies += spread(2)
-    loads[4].wait()
     loads[5].wait()
     own = []
     sources = (early_ref, cot_buf, late_ref)
@@ -147,7 +151,7 @@
         own.append(
             pltpu.make_async_copy(sources[a], token_pairs[a][1].at[mine], own_sem.at[a])
         )
-    for c, (block, whole) in enumerate(((gu_ref, gu_all), (dn_buf, dn_all))):
+    for c, (block, whole) in enumerate(((gu_ref, gu_all), (dn_ref, dn_all))):
         own.append(
             pltpu.make_async_copy(
                 block,
@@ -184,14 +188,14 @@
         copy.wait()
 
 
-def gather(n, n_tp, gate, up, dn, late, early, cot, gain):
-    rows, width = gate.shape
+def gather(n, n_tp, turned, gate, up, dn, late, early, cot, gain):
+    rows, width = gate.shape[::-1] if turned else gate.shape
     tokens, depth = late.shape
     vmem = pl.BlockSpec(memory_space=pltpu.VMEM)
     hbm = pl.BlockSpec(memory_space=pl.ANY)
     bf16 = jnp.bfloat16
     return pl.pallas_call(
-        functools.partial(gather_kernel, n, n_tp),
+        functools.partial(gather_kernel, n, n_tp, turned),
         out_shape=[
             jax.ShapeDtypeStruct((n * rows, 2 * width), bf16),
             jax.ShapeDtypeStruct((n * rows, width), bf16),
@@ -200,9 +204,10 @@
         in_specs=[hbm] * 6 + [vmem],
         out_specs=[hbm] * 5,
         scratch_shapes=[
-            pltpu.VMEM((rows, width), bf16),
-            pltpu.VMEM((rows, width), bf16),
+            pltpu.VMEM(gate.shape, bf16),
+            pltpu.VMEM(gate.shape, bf16),
             pltpu.VMEM((rows, 2 * width), bf16),
+            pltpu.VMEM(gate.shape, bf16),
             pltpu.VMEM((rows, width), bf16),
         ]
         + [pltpu.VMEM((tokens, depth), bf16)] * 5
@@ -220,17 +225,17 @@
     )(gate, up, dn, late, early, cot, gain)
 
 
-def reduce_kernel(n, n_tp, *refs):
-    gu_ref, dn_ref, both_ref, gain_ref, gu_in, dn_in, late_in, early_in = refs[:8]
-    gu_out, dn_out, mix_out, dnorm_out, gain_out = refs[8:13]
-    gu_slots, dn_slots, gain_slots, gain_tp = refs[13:17]
-    gu_all, dn_all, late_all, early_all, mix_ref, dnorm_ref, gain_sum = refs[17:24]
-    send_sem, recv_sem, gain_send, gain_recv, tp_send, tp_recv, last_send, last_recv = refs[24:32]
-    in_sem, own_sem = refs[32:]
+def reduce_kernel(n, n_tp, turned, *refs):
+    early_side, cot_side, both_ref, hid_ref, gain_ref, early_all, gu_in, dn_in, late_in = refs[:9]
+    gu_out, dn_out, mix_out, dnorm_out, gain_out = refs[9:14]
+    gu_slots, dn_slots, gain_slots, gain_tp, gu_first, dn_first = refs[14:20]
+    gu_all, dn_all, late_all, mix_ref, dnorm_ref, gain_sum = refs[20:26]
+    send_sem, recv_sem, gain_send, gain_recv, tp_send, tp_recv, last_send, last_recv = refs[26:34]
+    in_sem, own_sem = refs[34:]
     loads = [
         pltpu.make_async_copy(source, target, in_sem.at[k])
         for k, (source, target) in enumerate(
-            ((gu_in, gu_all), (early_in, early_all), (late_in, late_all), (dn_in, dn_all))
+            ((gu_in, gu_all), (late_in, late_all), (dn_in, dn_all))
         )
     ]
     for copy in loads:
@@ -250,10 +255,11 @@
         pl.semaphore_signal(barrier, inc=1, device_id=(me_fs, peer), device_id_type=MESH)
     pl.semaphore_wait(barrier, n - 1 + n_tp - 1)
     width = dn_all.shape[1]
-    rows = gu_ref.shape[0] // n
-    half = rows // 2
+    half = gu_first.shape[1]
+    rows = 2 * half
     tokens = late_all.shape[0] // n_tp
-    sets = ((gu_ref, gu_slots, gu_out), (dn_ref, dn_slots, dn_out))
+    sets = ((gu_first, gu_slots), (dn_first, dn_slots))
+    factors = ((early_side, both_ref, 1.0), (cot_side, hid_ref, 0.5))
 
     def local(step, way):
         if way == 0:
@@ -262,9 +268,22 @@
             owner = ring_index(lax.rem(place + step + 1, n), n)
         return pl.ds(pl.multiple_of(owner * rows + way * half, half), half)
 
+    def product(step, c, way):
+        side, other, factor = factors[c]
+        if turned:
+            left, contract = side[:, local(step, way)], 0
+        else:
+            left, contract = side[local(step, way), :], 1
+        return factor * lax.dot_general(
+            left,
+            other[...],
+            (((contract,), (0,)), ((), ())),
+            preferred_element_type=jnp.float32,
+        )
+
     def piece(step, c, way, first, landed=False):
-        partial, slots, _ = sets[c]
-        source = partial.at[local(0, way)] if first else slots.at[way, step if landed else step - 1]
+        start, slots = sets[c]
+        source = start.at[way] if first else slots.at[way, step if landed else step - 1]
         return pltpu.make_async_remote_copy(
             src_ref=source,
             dst_ref=slots.at[way, step],
@@ -331,6 +350,7 @@
 
     for c in range(2):
         for way in range(2):
+            sets[c][0][way] = product(0, c, way).astype(jnp.bfloat16)
             piece(0, c, way, True).start()
     gain_sum[...] = jnp.zeros_like(gain_sum)
     for copy in loads:
@@ -338,12 +358,12 @@
 
     def body(step, carry):
         for c in range(2):
-            partial, slots, _ = sets[c]
+            slots = sets[c][1]
             for way in range(2):
+                term = product(step, c, way)
                 piece(step - 1, c, way, False, True).wait_recv()
                 slots[way, step - 1] = (
-                    slots[way, step - 1].astype(jnp.float32)
-                    + partial[local(step, way), :].astype(jnp.float32)
+                    slots[way, step - 1].astype(jnp.float32) + term
                 ).astype(jnp.bfloat16)
                 piece(step, c, way, False).start()
 
@@ -395,12 +415,16 @@
         copy.start()
         last.append(copy)
     for c in range(2):
-        partial, slots, out = sets[c]
+        slots = sets[c][1]
         for way in range(2):
+            term = product(n - 1, c, way)
             piece(n - 2, c, way, False, True).wait_recv()
-            out[pl.ds(way * half, half), :] = slots[way, n - 2].astype(jnp.float32) + partial[
-                local(n - 1, way), :
-            ].astype(jnp.float32)
+            total = slots[way, n - 2].astype(jnp.float32) + term
+            out = (gu_out, dn_out)[c]
+            if turned:
+                out[:, pl.ds(way * half, half)] = total.T
+            else:
+                out[pl.ds(way * half, half), :] = total
             piece(0, c, way, True).wait_send()
     for copy in last:
         copy.wait()
@@ -422,34 +446,39 @@
             share(a, away).wait()
 
 
-def reduce(n, n_tp, gu, dn, both, gain, gu_all, dn_all, late_all, early_all):
-    rows = gu.shape[0] // n
+def reduce(n, n_tp, turned, early_side, cot_side, both, hid, gain, early_all, gu_all, dn_all, late_all):
+    rows = gu_all.shape[0] // n
     half = rows // 2
+    width = dn_all.shape[1]
+    shapes = [(rows, 2 * width), (rows, width)]
+    if turned:
+        shapes = [shape[::-1] for shape in shapes]
     depth = late_all.shape[1]
     tokens = late_all.shape[0] // n_tp
     vmem = pl.BlockSpec(memory_space=pltpu.VMEM)
     hbm = pl.BlockSpec(memory_space=pl.ANY)
     f32, bf16 = jnp.float32, jnp.bfloat16
     return pl.pallas_call(
-        functools.partial(reduce_kernel, n, n_tp),
+        functools.partial(reduce_kernel, n, n_tp, turned),
         out_shape=[
-            jax.ShapeDtypeStruct((rows, gu.shape[1]), f32),
-            jax.ShapeDtypeStruct((rows, dn.shape[1]), f32),
+            jax.ShapeDtypeStruct(shapes[0], f32),
+            jax.ShapeDtypeStruct(shapes[1], f32),
             jax.ShapeDtypeStruct((n_tp, tokens, depth), bf16),
             jax.ShapeDtypeStruct((n_tp, tokens, depth), bf16),
             jax.ShapeDtypeStruct(gain.shape, f32),
         ],
-        in_specs=[vmem] * 4 + [hbm] * 4,
+        in_specs=[vmem] * 6 + [hbm] * 3,
         out_specs=[vmem, vmem, hbm, hbm, vmem],
         scratch_shapes=[
-            pltpu.VMEM((2, n - 1, half, gu.shape[1]), bf16),
-            pltpu.VMEM((2, n - 1, half, dn.shape[1]), bf16),
+            pltpu.VMEM((2, n - 1, half, 2 * width), bf16),
+            pltpu.VMEM((2, n - 1, half, width), bf16),
             pltpu.VMEM((n,) + gain.shape, f32),
             pltpu.VMEM((n_tp,) + gain.shape, f32),
+            pltpu.VMEM((2, half, 2 * width), bf16),
+            pltpu.VMEM((2, half, width), bf16),
             pltpu.VMEM(gu_all.shape, bf16),
             pltpu.VMEM(dn_all.shape, bf16),
             pltpu.VMEM(late_all.shape, bf16),
-            pltpu.VMEM(early_all.shape, bf16),
             pltpu.VMEM((n_tp, tokens, depth), bf16),
             pltpu.VMEM((n_tp, tokens, depth), bf16),
             pltpu.VMEM(gain.shape, f32),
@@ -461,19 +490,13 @@
             pltpu.SemaphoreType.DMA((2, n_tp - 1)),
             pltpu.SemaphoreType.DMA((n_tp - 1,)),
             pltpu.SemaphoreType.DMA((n_tp - 1,)),
-            pltpu.SemaphoreType.DMA((4,)),
+            pltpu.SemaphoreType.DMA((3,)),
             pltpu.SemaphoreType.DMA((2,)),
         ],
         compiler_params=pltpu.CompilerParams(
             collective_id=1, has_side_effects=True, vmem_limit_bytes=VMEM_LIMIT
         ),
-    )(gu, dn, both, gain, gu_all, dn_all, late_all, early_all)
-
-
-def column_product(left, right):
-    return lax.dot_general(
-        left, right, (((0,), (0,)), ((), ())), preferred_element_type=jnp.float32
-    )
+    )(early_side, cot_side, both, hid, gain, early_all, gu_all, dn_all, late_all)
 
 
 def per_device(
@@ -494,9 +517,13 @@
     gain_f = norm_gain.astype(jnp.float32)
     width = gate_weight.shape[1]
     depth = late_input.shape[1]
+    turned = gate_weight.shape[0] % 256 == 0
+    weights = [gate_weight, up_weight, down_weight]
+    if turned:
+        weights = [weight.T for weight in weights]
     gain_row = gain_f.reshape(1, depth)
     gu_all, down_all, late_all, early_all, cot_all = gather(
-        n, n_tp, gate_weight, up_weight, down_weight, late_input, early_input, cotangent, gain_row
+        n, n_tp, turned, *weights, late_input, early_input, cotangent, gain_row
     )
     both_e = jnp.dot(early_all, gu_all, preferred_element_type=jnp.float32)
     gate_e, upper_e = both_e[:, :width], both_e[:, width:]
@@ -506,11 +533,14 @@
     d_gate = (d_hidden * upper_e * sigma_e * (1.0 + gate_e * (1.0 - sigma_e))).astype(jnp.bfloat16)
     d_up = (d_hidden * gate_e * sigma_e).astype(jnp.bfloat16)
     d_both = jnp.concatenate([d_gate, d_up], axis=1)
-    gu_part = column_product(early_all, d_both).astype(jnp.bfloat16)
-    down_part = (0.5 * column_product(cot_all, hidden_e)).astype(jnp.bfloat16)
+    sides = (early_all, cot_all) if turned else (early_all.T, cot_all.T)
     gu_grad, down_grad, mix_got, d_got, gain_total = reduce(
-        n, n_tp, gu_part, down_part, d_both, gain_row, gu_all, down_all, late_all, early_all
+        n, n_tp, turned, *sides, d_both, hidden_e, gain_row, early_all, gu_all, down_all, late_all
     )
+    if turned:
+        gate_grad, up_grad, down_grad = gu_grad[:width].T, gu_grad[width:].T, down_grad.T
+    else:
+        gate_grad, up_grad = gu_grad[:, :width], gu_grad[:, width:]
 
     def gathered(got):
         total = got[0].astype(jnp.float32)
@@ -531,8 +561,8 @@
     return (
         late_out,
         early_grad,
-        gate_sum + gu_grad[:, :width],
-        up_sum + gu_grad[:, width:],
+        gate_sum + gate_grad,
+        up_sum + up_grad,
         down_sum + down_grad,
         gain_sum + gain_total.reshape(depth),
     )

time: 228 us -> 208 us (0.912)
  local copies, waits for them, and re-layouts: 11.9 us -> 0.18 us
  matrix products: 17.8 us -> 9.71 us
    unnamed x35 -> x28, local copies, waits for them, and re-layouts: 11.9 us -> 0.18 us
    dot_general x2 -> x0, matrix products: 9.01 us -> none  [column_product(): lax.dot_general(left, right, (((0,), (0,)), ((), ())), preferred_element_...]
where the time goes in v3:
time: 208 us
  Pallas kernels  187 us (90%)
  other arithmetic  10.1 us (5%)
  matrix products  9.71 us (5%)
    pallas_call x1, Pallas kernels, reduce(): pl.pallas_call(functools.partial(reduce_kernel, n, n_tp, turned), out_sha...  96.3 us
    pallas_call x1, Pallas kernels, gather(): pl.pallas_call(functools.partial(gather_kernel, n, n_tp, turned), out_sha...  90.9 us
    dot_general x1, matrix products, per_device(): both_e = jnp.dot(early_all, gu_all, preferred_element_type=jnp.float32)  6.54 us

profile of v3, /device:TPU:0, one launch (start us, length us, event | category | flops | bytes accessed | tf_op | source)
XLA Modules:
  0.0 208.1 jit_solution(10760820029383968018)
XLA Ops:
  0.6 1.3 convert_element_type.60
  1.9 90.9 %shard_map.154 = (bf16[2048,1408]{1,0:T(8,128)(2,1)}, bf16[2048,704]{1,0:T(8,128)(2,1)}, bf16[512,2048]{1,0:T(8,128)(2,1)}, bf16[512,2048]{1,0:T(8,128)(2,1)}, bf16[512,2048]{1,0:T(8,128)(2,1)}) custom-call(bf16[704,256]{1,0:T(8,128)(2,1)} %bitcast.25, bf16[704,256]{1,0:T(8,128)(2,1)} %bitcast.26, bf16[704,256]{1,0:T(8,128)(2,1)} %bitcast.27, ...), custom_call_target="tpu_custom_call" | custom-call | tf_op jit(solution)/shard_map/pallas_call | solution.py:197
  92.8 0.0 copy-start.2
  92.8 0.0 copy-start.3
  92.9 6.5 %fusion.6 = f32[512,1408]{1,0:T(8,128)S(1)} fusion(bf16[512,2048]{1,0:T(8,128)(2,1)} %get-tuple-element.16.refs_0_.refs_5_, bf16[2048,1408]{1,0:T(8,128)(2,1)} %get-tuple-element.19.refs_6_), kind=kOutput, calls=%fused_computation.23 | convolution fusion | flops 2952790016 | bytes 10747904 | tf_op jit(solution)/shard_map/dot_general | solution.py:528
  99.4 0.0 copy-done.2
  99.4 0.0 copy-done.3
  99.4 3.2 %multiply_convert_fusion.2 = (bf16[512,704]{1,0:T(8,128)(2,1)S(1)}, bf16[512,704]{1,0:T(8,128)(2,1)S(1)}, bf16[512,704]{1,0:T(8,128)(2,1)}) fusion(f32[512,1408]{1,0:T(8,128)S(1)} %fusion.6, bf16[512,2048]{1,0:T(8,128)(2,1)S(1)} %copy-done.3, bf16[2048,704]{1,0:T(8,128)(2,1)S(1)} %copy-done.2), kind=kOutput, calls=%fused_computation.5 | convolution fusion | flops 1482522624 | bytes 10027008 | tf_op jit(solution)/shard_map/dot_general | solution.py:532
  102.6 1.5 pad_maximum_fusion.refs_2_
  104.1 96.3 %shard_map.155 = (f32[1408,256]{1,0:T(8,128)}, f32[704,256]{1,0:T(8,128)}, bf16[4,128,2048]{2,1,0:T(8,128)(2,1)}, bf16[4,128,2048]{2,1,0:T(8,128)(2,1)}, f32[1,2048]{1,0:T(1,128)}) custom-call(bf16[512,2048]{1,0:T(8,128)(2,1)} %get-tuple-element.16.refs_0_.refs_5_, bf16[512,2048]{1,0:T(8,128)(2,1)} %get-tuple-element.17.refs_1_, ...), custom_call_target="tpu_custom_call" | custom-call | tf_op jit(solution)/shard_map/pallas_call | solution.py:461
  200.5 0.0 copy-done.1
  200.5 0.0 copy-done.4
  200.5 0.0 copy-done.11
  200.5 0.0 copy-start
  200.5 0.0 copy-start.5
  200.5 0.0 copy-start.10
  200.5 3.9 %fusion = (f32[128]{0:T(128)S(1)}, f32[128]{0:T(128)S(1)}, bf16[128,2048]{1,0:T(8,128)(2,1)}) fusion(bf16[128,2048]{1,0:T(8,128)(2,1)S(1)} %copy-done.1, f32[2048]{0:T(1024)S(1)} %copy-done.11, bf16[4,128,2048]{2,1,0:T(8,128)(2,1)} %get-tuple-element.22, bf16[4,128,2048]{2,1,0:T(8,128)(2,1)} %get-tuple-element.21, bf16[128,2048]{1,0:T(8,128)(2,1)S(1)} %copy-done.4), kind=kLoop, calls=%fused_computation.9 | loop fusion | flops 6291200 | bytes 5776384 | tf_op jit(solution)/shard_map/reduce_sum | solution.py:553
  204.5 0.0 copy-start.7
  204.5 0.0 copy-start.8
  204.5 0.0 copy-start.9
  204.5 0.0 copy-done
  204.5 0.0 copy-done.5
  204.6 1.4 fusion.3
  205.9 0.0 copy-done.12
  205.9 0.0 copy-done.13
  205.9 0.6 add.83
  206.5 0.0 copy-done.10
  206.5 0.0 copy-done.6
  206.5 0.0 copy-done.7
  206.5 0.0 copy-done.8
  206.5 0.1 copy-done.9
  206.7 1.4 bitcast_add_fusion.2
  (8 shorter events, 0.0 us)
Async XLA Ops:
  92.8 6.6 %copy-start.2 = (bf16[2048,704]{1,0:T(8,128)(2,1)S(1)}, bf16[2048,704]{1,0:T(8,128)(2,1)}, u32[]{:S(2)}) copy-start(bf16[2048,704]{1,0:T(8,128)(2,1)} %get-tuple-element.18.refs_7_) | copy-start | bytes 8650756
  92.8 6.6 %copy-start.3 = (bf16[512,2048]{1,0:T(8,128)(2,1)S(1)}, bf16[512,2048]{1,0:T(8,128)(2,1)}, u32[]{:S(2)}) copy-start(bf16[512,2048]{1,0:T(8,128)(2,1)} %get-tuple-element.17.refs_1_) | copy-start | bytes 6291460
  104.1 96.4 %copy-start.1 = (bf16[128,2048]{1,0:T(8,128)(2,1)S(1)}, bf16[128,2048]{1,0:T(8,128)(2,1)}, u32[]{:S(2)}) copy-start(bf16[128,2048]{1,0:T(8,128)(2,1)} %refs_4_.1) | copy-start | bytes 1572868
  104.1 96.4 %copy-start.4 = (bf16[128,2048]{1,0:T(8,128)(2,1)S(1)}, bf16[128,2048]{1,0:T(8,128)(2,1)}, u32[]{:S(2)}) copy-start(bf16[128,2048]{1,0:T(8,128)(2,1)} %refs_3_.1) | copy-start | bytes 1572868
  104.1 96.4 %copy-start.11 = (f32[2048]{0:T(1024)S(1)}, f32[2048]{0:T(1024)}, u32[]{:S(2)}) copy-start(f32[2048]{0:T(1024)} %convert_element_type.60) | copy-start | bytes 24580
  200.5 4.0 %copy-start = (bf16[4,128,2048]{2,1,0:T(8,128)(2,1)S(1)}, bf16[4,128,2048]{2,1,0:T(8,128)(2,1)}, u32[]{:S(2)}) copy-start(bf16[4,128,2048]{2,1,0:T(8,128)(2,1)} %get-tuple-element.22) | copy-start | bytes 6291460
  200.5 4.0 %copy-start.5 = (bf16[128,2048]{1,0:T(8,128)(2,1)S(1)}, bf16[128,2048]{1,0:T(8,128)(2,1)}, u32[]{:S(2)}) copy-start(bf16[128,2048]{1,0:T(8,128)(2,1)} %refs_5_.1) | copy-start | bytes 1572868
  200.5 6.0 %copy-start.10 = (f32[704,256]{1,0:T(8,128)S(1)}, f32[704,256]{1,0:T(8,128)}, u32[]{:S(2)}) copy-start(f32[704,256]{1,0:T(8,128)} %get-tuple-element.24) | copy-start | bytes 2162692
  204.5 1.5 copy-start.12
  204.5 1.5 copy-start.13
  204.5 2.1 copy-start.6
  204.5 2.1 copy-start.7
  204.5 2.1 copy-start.8
  204.5 2.2 %copy-start.9 = (f32[256,704]{0,1:T(8,128)S(1)}, f32[256,704]{0,1:T(8,128)}, u32[]{:S(2)}) copy-start(f32[256,704]{0,1:T(8,128)} %param.20) | copy-start | bytes 2162692

commit v4 on v3

--- a/solution.py
+++ b/solution.py
@@ -45,10 +45,13 @@
 
 def gather_kernel(n, n_tp, turned, *refs):
     gate_in, up_in, dn_in, late_in, early_in, cot_ref, gain_ref = refs[:7]
-    gu_all, dn_all, late_all, early_all, cot_all = refs[7:12]
-    gate_buf, up_buf, gu_ref, dn_buf, dn_ref = refs[12:17]
-    late_buf, early_buf, cot_buf, late_ref, early_ref = refs[17:22]
-    send_sem, recv_sem, tp_send, tp_recv, own_sem, in_sem = refs[22:]
+    gu_out, dn_out, late_all, early_out, cot_out, both_out, hid_out = refs[7:14]
+    gate_buf, up_buf, gu_ref, dn_buf, dn_ref, late_buf, early_buf, late_ref = refs[14:22]
+    gu_all, dn_all, early_all, cot_all, sum_gu, sum_dn = refs[22:28]
+    send_sem, recv_sem, tp_send, tp_recv, own_sem, in_sem, out_sem = refs[28:]
+    me_fs, me_tp = lax.axis_index("fs"), lax.axis_index("tp")
+    tokens = late_in.shape[0]
+    mine = pl.ds(pl.multiple_of(me_tp * tokens, tokens), tokens)
     rows, width = dn_ref.shape
     loads = [
         pltpu.make_async_copy(source, target, in_sem.at[k])
@@ -59,17 +62,16 @@
                 (early_in, early_buf),
                 (late_in, late_buf),
                 (dn_in, dn_buf),
-                (cot_ref, cot_buf),
+                (cot_ref, cot_all.at[mine]),
             )
         )
     ]
     for copy in loads:
         copy.start()
-    me_fs, me_tp = lax.axis_index("fs"), lax.axis_index("tp")
     place, right, left = neighbours(n)
     greet(n_tp, right, left)
     half = rows // 2
-    tokens = late_in.shape[0]
+    outs = (gu_out, dn_out)
     pairs = ((gu_ref, gu_all), (dn_ref, dn_all))
 
     def window(owner, way):
@@ -94,32 +96,58 @@
             device_id_type=MESH,
         )
 
-    mine = pl.ds(pl.multiple_of(me_tp * tokens, tokens), tokens)
-    token_pairs = ((early_ref, early_all), (cot_ref, cot_all), (late_ref, late_all))
+    token_pairs = (
+        (early_all.at[mine], early_all),
+        (cot_ref, cot_all),
+        (late_ref, late_all),
+    )
+
+    def token_piece(a, away):
+        block, whole = token_pairs[a]
+        return pltpu.make_async_remote_copy(
+            src_ref=block,
+            dst_ref=whole.at[mine],
+            send_sem=tp_send.at[a, away - 1],
+            recv_sem=tp_recv.at[a, away - 1],
+            device_id=(me_fs, lax.rem(me_tp + away, n_tp)),
+            device_id_type=MESH,
+        )
 
     def spread(a):
-        block, whole = token_pairs[a]
-        copies = []
         for away in range(1, n_tp):
-            peer = lax.rem(me_tp + away, n_tp)
-            copy = pltpu.make_async_remote_copy(
-                src_ref=block,
-                dst_ref=whole.at[mine],
-                send_sem=tp_send.at[a, away - 1],
-                recv_sem=tp_recv.at[a, away - 1],
-                device_id=(me_fs, peer),
-                device_id_type=MESH,
+            token_piece(a, away).start()
+
+    def arrived(a):
+        for away in range(1, n_tp):
+            token_piece(a, away).wait()
+
+    def owner_of(step, way):
+        if way == 0:
+            return ring_index(lax.rem(place - step + n, n), n)
+        return ring_index(lax.rem(place + step, n), n)
+
+    def landed(step, c, way):
+        some = window(owner_of(step + 1, way), way)
+        return pltpu.make_async_copy(
+            pairs[c][1].at[some], outs[c].at[some], out_sem.at[step, c, way]
+        )
+
+    totals = ((sum_gu, early_all), (sum_dn, cot_all))
+
+    def add_rows(step, c):
+        total, left = totals[c]
+        for way in range(2):
+            some = window(owner_of(step, way), way)
+            total[...] += jnp.dot(
+                left[:, some], pairs[c][1][some, :], preferred_element_type=jnp.float32
             )
-            copy.start()
-            copies.append(copy)
-        return copies
-
-    def norm(source, target):
+
+    def norm(source, target, base):
         def part(k, carry):
             some = pl.ds(pl.multiple_of(k * 16, 16), 16)
             values = source[some, :].astype(jnp.float32)
             scale = lax.rsqrt(jnp.mean(values * values, axis=-1, keepdims=True) + epsilon)
-            target[some, :] = (values * scale * gain_ref[...]).astype(jnp.bfloat16)
+            target[pl.ds(pl.multiple_of(base + k * 16, 16), 16), :] = (values * scale * gain_ref[...]).astype(jnp.bfloat16)
             return carry
 
         lax.fori_loop(0, tokens // 16, part, 0)
@@ -131,7 +159,6 @@
     dn_ref[...] = plain(dn_buf)
     for way in range(2):
         piece(0, 1, way, True).start()
-    token_copies = spread(1)
     loads[0].wait()
     loads[1].wait()
     gu_ref[:, :width] = plain(gate_buf)
@@ -139,41 +166,82 @@
     for way in range(2):
         piece(0, 0, way, True).start()
     loads[2].wait()
-    norm(early_buf, early_ref)
-    token_copies += spread(0)
+    norm(early_buf, early_all, me_tp * tokens)
+    spread(0)
+    spread(1)
     loads[3].wait()
-    norm(late_buf, late_ref)
-    token_copies += spread(2)
+    norm(late_buf, late_ref, 0)
+    spread(2)
     loads[5].wait()
-    own = []
-    sources = (early_ref, cot_buf, late_ref)
-    for a in range(3):
-        own.append(
-            pltpu.make_async_copy(sources[a], token_pairs[a][1].at[mine], own_sem.at[a])
-        )
-    for c, (block, whole) in enumerate(((gu_ref, gu_all), (dn_ref, dn_all))):
-        own.append(
-            pltpu.make_async_copy(
-                block,
-                whole.at[pl.ds(pl.multiple_of(me_fs * rows, rows), rows)],
-                own_sem.at[3 + c],
-            )
-        )
+    here = pl.ds(pl.multiple_of(me_fs * rows, rows), rows)
+    gu_all[here, :] = gu_ref[...]
+    dn_all[here, :] = dn_ref[...]
+    sum_gu[...] = jnp.zeros_like(sum_gu)
+    sum_dn[...] = jnp.zeros_like(sum_dn)
+    own = [
+        pltpu.make_async_copy(late_ref, late_all.at[mine], own_sem.at[0]),
+        pltpu.make_async_copy(gu_ref, gu_out.at[here], own_sem.at[1]),
+        pltpu.make_async_copy(dn_ref, dn_out.at[here], own_sem.at[2]),
+    ]
     for copy in own:
         copy.start()
+    keep = [
+        pltpu.make_async_copy(early_all, early_out, own_sem.at[3]),
+        pltpu.make_async_copy(cot_all, cot_out, own_sem.at[4]),
+    ]
 
     def body(step, carry):
         for c in (1, 0):
             for way in range(2):
                 piece(step - 1, c, way, False).wait_recv()
                 piece(step, c, way, False).start()
+                landed(step - 1, c, way).start()
+            which = 1 - c
+
+            @pl.when(step == n // 2)
+            def _():
+                arrived(which)
+                keep[which].start()
+
+            if turned:
+
+                @pl.when(step >= n // 2)
+                def _():
+                    add_rows(2 * (step - n // 2), which)
+                    add_rows(2 * (step - n // 2) + 1, which)
+
         return carry
 
     lax.fori_loop(1, n - 1, body, 0)
+    if turned:
+        for c in (1, 0):
+            add_rows(n - 2, c)
     for c in (1, 0):
         for way in range(2):
             piece(n - 2, c, way, False).wait_recv()
+            landed(n - 2, c, way).start()
             piece(0, c, way, True).wait_send()
+        if turned:
+            add_rows(n - 1, c)
+        else:
+            total, rest = totals[c]
+            total[...] = jnp.dot(
+                rest[...], pairs[c][1][...], preferred_element_type=jnp.float32
+            )
+
+    def finish(k, carry):
+        some = pl.ds(pl.multiple_of(k * 16, 16), 16)
+        gate, upper = sum_gu[some, :width], sum_gu[some, width:]
+        sigma = 1.0 / (1.0 + jnp.exp(-gate))
+        d_hidden = 0.5 * sum_dn[some, :]
+        hid_out[some, :] = (gate * sigma * upper).astype(jnp.bfloat16)
+        both_out[some, :width] = (
+            d_hidden * upper * sigma * (1.0 + gate * (1.0 - sigma))
+        ).astype(jnp.bfloat16)
+        both_out[some, width:] = (d_hidden * gate * sigma).astype(jnp.bfloat16)
+        return carry
+
+    lax.fori_loop(0, n_tp * tokens // 16, finish, 0)
 
     def drain(step, carry):
         for c in (1, 0):
@@ -182,10 +250,17 @@
         return carry
 
     lax.fori_loop(1, n - 1, drain, 0)
-    for copy in own:
+
+    def put(step, carry):
+        for c in range(2):
+            for way in range(2):
+                landed(step, c, way).wait()
+        return carry
+
+    lax.fori_loop(0, n - 1, put, 0)
+    for copy in own + keep:
         copy.wait()
-    for copy in token_copies:
-        copy.wait()
+    arrived(2)
 
 
 def gather(n, n_tp, turned, gate, up, dn, late, early, cot, gain):
@@ -200,9 +275,13 @@
             jax.ShapeDtypeStruct((n * rows, 2 * width), bf16),
             jax.ShapeDtypeStruct((n * rows, width), bf16),
         ]
-        + [jax.ShapeDtypeStruct((n_tp * tokens, depth), bf16)] * 3,
+        + [jax.ShapeDtypeStruct((n_tp * tokens, depth), bf16)] * 3
+        + [
+            jax.ShapeDtypeStruct((n_tp * tokens, 2 * width), bf16),
+            jax.ShapeDtypeStruct((n_tp * tokens, width), bf16),
+        ],
         in_specs=[hbm] * 6 + [vmem],
-        out_specs=[hbm] * 5,
+        out_specs=[hbm] * 5 + [vmem] * 2,
         scratch_shapes=[
             pltpu.VMEM(gate.shape, bf16),
             pltpu.VMEM(gate.shape, bf16),
@@ -210,7 +289,15 @@
             pltpu.VMEM(gate.shape, bf16),
             pltpu.VMEM((rows, width), bf16),
         ]
-        + [pltpu.VMEM((tokens, depth), bf16)] * 5
+        + [pltpu.VMEM((tokens, depth), bf16)] * 3
+        + [
+            pltpu.VMEM((n * rows, 2 * width), bf16),
+            pltpu.VMEM((n * rows, width), bf16),
+            pltpu.VMEM((n_tp * tokens, depth), bf16),
+            pltpu.VMEM((n_tp * tokens, depth), bf16),
+            pltpu.VMEM((n_tp * tokens, 2 * width), jnp.float32),
+            pltpu.VMEM((n_tp * tokens, width), jnp.float32),
+        ]
         + [
             pltpu.SemaphoreType.DMA((n - 1, 2, 2)),
             pltpu.SemaphoreType.DMA((n - 1, 2, 2)),
@@ -218,6 +305,7 @@
             pltpu.SemaphoreType.DMA((3, n_tp - 1)),
             pltpu.SemaphoreType.DMA((5,)),
             pltpu.SemaphoreType.DMA((6,)),
+            pltpu.SemaphoreType.DMA((n - 1, 2, 2)),
         ],
         compiler_params=pltpu.CompilerParams(
             collective_id=0, has_side_effects=True, vmem_limit_bytes=VMEM_LIMIT
@@ -356,6 +444,10 @@
     for copy in loads:
         copy.wait()
 
+    for c in range(2):
+        (grad_block, late_block)[c](1)
+        share(c, 1).start()
+
     def body(step, carry):
         for c in range(2):
             slots = sets[c][1]
@@ -367,19 +459,19 @@
                 ).astype(jnp.bfloat16)
                 piece(step, c, way, False).start()
 
-            @pl.when(step <= n_tp)
-            def _():
-                (grad_block, late_block)[c](step)
-
             @pl.when(step < n_tp)
             def _():
-                share(c, step).start()
-
-            @pl.when(step == n_tp)
+                (grad_block, late_block)[c](step + 1)
+
+            @pl.when(step < n_tp - 1)
+            def _():
+                share(c, step + 1).start()
+
+            @pl.when(step == n_tp - 1)
             def _():
                 keep(c).start()
 
-        @pl.when(step == n_tp)
+        @pl.when(step == n_tp - 1)
         def _():
             gain_slots[me_fs] = gain_sum[...] / gain_ref[...]
 
@@ -522,17 +614,9 @@
     if turned:
         weights = [weight.T for weight in weights]
     gain_row = gain_f.reshape(1, depth)
-    gu_all, down_all, late_all, early_all, cot_all = gather(
+    gu_all, down_all, late_all, early_all, cot_all, d_both, hidden_e = gather(
         n, n_tp, turned, *weights, late_input, early_input, cotangent, gain_row
     )
-    both_e = jnp.dot(early_all, gu_all, preferred_element_type=jnp.float32)
-    gate_e, upper_e = both_e[:, :width], both_e[:, width:]
-    sigma_e = jax.nn.sigmoid(gate_e)
-    hidden_e = (gate_e * sigma_e * upper_e).astype(jnp.bfloat16)
-    d_hidden = 0.5 * jnp.dot(cot_all, down_all, preferred_element_type=jnp.float32)
-    d_gate = (d_hidden * upper_e * sigma_e * (1.0 + gate_e * (1.0 - sigma_e))).astype(jnp.bfloat16)
-    d_up = (d_hidden * gate_e * sigma_e).astype(jnp.bfloat16)
-    d_both = jnp.concatenate([d_gate, d_up], axis=1)
     sides = (early_all, cot_all) if turned else (early_all.T, cot_all.T)
     gu_grad, down_grad, mix_got, d_got, gain_total = reduce(
         n, n_tp, turned, *sides, d_both, hidden_e, gain_row, early_all, gu_all, down_all, late_all

time: 208 us -> 203 us (0.976)
  matrix products: 9.71 us -> 0 us
  Pallas kernels: 187 us -> 193 us
    dot_general x2 -> x0, matrix products: 9.71 us -> none  [the longest x1 6.54 us: per_device(): both_e = jnp.dot(early_all, gu_all, preferred_element_type=jnp.float32)]
    pallas_call x1, Pallas kernels: 90.9 us -> 96.7 us  [gather(): pl.pallas_call(functools.partial(gather_kernel, n, n_tp, turned), out_sha...]
where the time goes in v4:
time: 203 us
  Pallas kernels  193 us (95%)
  other arithmetic  8.6 us (4%)
    pallas_call x1, Pallas kernels, gather(): pl.pallas_call(functools.partial(gather_kernel, n, n_tp, turned), out_sha...  96.7 us
    pallas_call x1, Pallas kernels, reduce(): pl.pallas_call(functools.partial(reduce_kernel, n, n_tp, turned), out_sha...  96.4 us

profile of v4, /device:TPU:0, one launch (start us, length us, event | category | flops | bytes accessed | tf_op | source)
XLA Modules:
  0.0 202.6 jit_solution(6153531800993761009)
XLA Ops:
  0.6 1.3 convert_element_type.51
  1.9 96.7 %shard_map.154 = (bf16[2048,1408]{1,0:T(8,128)(2,1)}, bf16[2048,704]{1,0:T(8,128)(2,1)}, bf16[512,2048]{1,0:T(8,128)(2,1)}, bf16[512,2048]{1,0:T(8,128)(2,1)}, b...) custom-call(bf16[704,256]{1,0:T(8,128)(2,1)} %bitcast.21, ...), custom_call_target="tpu_custom_call" | custom-call | tf_op jit(solution)/shard_map/pallas_call | solution.py:272
  98.6 0.0 copy-start.1
  98.6 0.0 copy-start.2
  98.6 0.0 copy-start.9
  98.6 96.4 %shard_map.155 = (f32[1408,256]{1,0:T(8,128)}, f32[704,256]{1,0:T(8,128)}, bf16[4,128,2048]{2,1,0:T(8,128)(2,1)}, bf16[4,128,2048]{2,1,0:T(8,128)(2,1)}, f32[1,2048]{1,0:T(1,128)}) custom-call(bf16[512,2048]{1,0:T(8,128)(2,1)} %get-tuple-element.18.refs_0_.refs_5_, bf16[512,2048]{1,0:T(8,128)(2,1)} %get-tuple-element.19.refs_1_, ...), custom_call_target="tpu_custom_call" | custom-call | tf_op jit(solution)/shard_map/pallas_call | solution.py:553
  195.0 0.0 copy-done.1
  195.0 0.0 copy-done.2
  195.0 0.0 copy-done.9
  195.0 0.0 copy-start
  195.0 0.0 copy-start.3
  195.0 0.0 copy-start.8
  195.0 3.9 %fusion = (f32[128]{0:T(128)S(1)}, f32[128]{0:T(128)S(1)}, bf16[128,2048]{1,0:T(8,128)(2,1)}) fusion(bf16[128,2048]{1,0:T(8,128)(2,1)S(1)} %copy-done.1, f32[2048]{0:T(1024)S(1)} %copy-done.9, bf16[4,128,2048]{2,1,0:T(8,128)(2,1)} %get-tuple-element.26, bf16[4,128,2048]{2,1,0:T(8,128)(2,1)} %get-tuple-element.25, bf16[128,2048]{1,0:T(8,128)(2,1)S(1)} %copy-done.2), kind=kLoop, calls=%fused_computation.3 | loop fusion | flops 6291200 | bytes 5776384 | tf_op jit(solution)/shard_map/reduce_sum | solution.py:637
  199.0 0.0 copy-start.10
  199.0 0.0 copy-start.11
  199.0 0.0 copy-start.4
  199.0 0.0 copy-start.5
  199.0 0.0 copy-start.6
  199.0 0.0 copy-start.7
  199.0 0.0 copy-done
  199.0 0.0 copy-done.3
  199.1 1.4 fusion.3
  200.4 0.0 copy-done.10
  200.4 0.0 copy-done.11
  200.4 0.6 add.75
  201.0 0.0 copy-done.8
  201.0 0.0 copy-done.4
  201.0 0.0 copy-done.5
  201.0 0.0 copy-done.6
  201.0 0.1 copy-done.7
  201.2 1.4 bitcast_add_fusion.2
  (2 shorter events, 0.0 us)
Async XLA Ops:
  98.6 96.4 %copy-start.1 = (bf16[128,2048]{1,0:T(8,128)(2,1)S(1)}, bf16[128,2048]{1,0:T(8,128)(2,1)}, u32[]{:S(2)}) copy-start(bf16[128,2048]{1,0:T(8,128)(2,1)} %refs_4_.1) | copy-start | bytes 1572868
  98.6 96.4 %copy-start.2 = (bf16[128,2048]{1,0:T(8,128)(2,1)S(1)}, bf16[128,2048]{1,0:T(8,128)(2,1)}, u32[]{:S(2)}) copy-start(bf16[128,2048]{1,0:T(8,128)(2,1)} %refs_3_.1) | copy-start | bytes 1572868
  98.6 96.4 %copy-start.9 = (f32[2048]{0:T(1024)S(1)}, f32[2048]{0:T(1024)}, u32[]{:S(2)}) copy-start(f32[2048]{0:T(1024)} %convert_element_type.51) | copy-start | bytes 24580
  195.0 4.0 %copy-start = (bf16[4,128,2048]{2,1,0:T(8,128)(2,1)S(1)}, bf16[4,128,2048]{2,1,0:T(8,128)(2,1)}, u32[]{:S(2)}) copy-start(bf16[4,128,2048]{2,1,0:T(8,128)(2,1)} %get-tuple-element.26) | copy-start | bytes 6291460
  195.0 4.0 %copy-start.3 = (bf16[128,2048]{1,0:T(8,128)(2,1)S(1)}, bf16[128,2048]{1,0:T(8,128)(2,1)}, u32[]{:S(2)}) copy-start(bf16[128,2048]{1,0:T(8,128)(2,1)} %refs_5_.1) | copy-start | bytes 1572868
  195.0 6.0 %copy-start.8 = (f32[704,256]{1,0:T(8,128)S(1)}, f32[704,256]{1,0:T(8,128)}, u32[]{:S(2)}) copy-start(f32[704,256]{1,0:T(8,128)} %get-tuple-element.28) | copy-start | bytes 2162692
  199.0 1.5 copy-start.10
  199.0 1.5 copy-start.11
  199.0 2.1 %copy-start.4 = (f32[1408,256]{1,0:T(8,128)S(1)}, f32[1408,256]{1,0:T(8,128)}, u32[]{:S(2)}) copy-start(f32[1408,256]{1,0:T(8,128)} %get-tuple-element.27) | copy-start | bytes 4325380
  199.0 2.1 %copy-start.5 = (f32[256,704]{0,1:T(8,128)S(1)}, f32[256,704]{0,1:T(8,128)}, u32[]{:S(2)}) copy-start(f32[256,704]{0,1:T(8,128)} %param.19) | copy-start | bytes 2162692
  199.0 2.1 %copy-start.6 = (f32[256,704]{0,1:T(8,128)S(1)}, f32[256,704]{0,1:T(8,128)}, u32[]{:S(2)}) copy-start(f32[256,704]{0,1:T(8,128)} %param.18) | copy-start | bytes 2162692
  199.0 2.2 %copy-start.7 = (f32[256,704]{0,1:T(8,128)S(1)}, f32[256,704]{0,1:T(8,128)}, u32[]{:S(2)}) copy-start(f32[256,704]{0,1:T(8,128)} %param.20) | copy-start | bytes 2162692

commit v5 on v4

--- a/solution.py
+++ b/solution.py
@@ -230,7 +230,7 @@
             )
 
     def finish(k, carry):
-        some = pl.ds(pl.multiple_of(k * 16, 16), 16)
+        some = pl.ds(pl.multiple_of(k * 64, 64), 64)
         gate, upper = sum_gu[some, :width], sum_gu[some, width:]
         sigma = 1.0 / (1.0 + jnp.exp(-gate))
         d_hidden = 0.5 * sum_dn[some, :]
@@ -241,7 +241,7 @@
         both_out[some, width:] = (d_hidden * gate * sigma).astype(jnp.bfloat16)
         return carry
 
-    lax.fori_loop(0, n_tp * tokens // 16, finish, 0)
+    lax.fori_loop(0, n_tp * tokens // 64, finish, 0)
 
     def drain(step, carry):
         for c in (1, 0):

time: 203 us -> 201 us (level)
  no operation moved by 1% of the time
where the time goes in v5:
time: 201 us
  Pallas kernels  191 us (95%)
  other arithmetic  8.6 us (4%)
    pallas_call x1, Pallas kernels, reduce(): pl.pallas_call(functools.partial(reduce_kernel, n, n_tp, turned), out_sha...  96.4 us
    pallas_call x1, Pallas kernels, gather(): pl.pallas_call(functools.partial(gather_kernel, n, n_tp, turned), out_sha...  94.6 us

profile of v5, /device:TPU:0, one launch (start us, length us, event | category | flops | bytes accessed | tf_op | source)
XLA Modules:
  0.0 200.6 jit_solution(638439002386993822)
XLA Ops:
  0.6 1.3 convert_element_type.51
  1.9 94.6 %shard_map.154 = (bf16[2048,1408]{1,0:T(8,128)(2,1)}, bf16[2048,704]{1,0:T(8,128)(2,1)}, bf16[512,2048]{1,0:T(8,128)(2,1)}, bf16[512,2048]{1,0:T(8,128)(2,1)}, b...) custom-call(bf16[704,256]{1,0:T(8,128)(2,1)} %bitcast.21, ...), custom_call_target="tpu_custom_call" | custom-call | tf_op jit(solution)/shard_map/pallas_call | solution.py:272
  96.6 0.0 copy-start.1
  96.6 0.0 copy-start.2
  96.6 0.0 copy-start.9
  96.6 96.4 %shard_map.155 = (f32[1408,256]{1,0:T(8,128)}, f32[704,256]{1,0:T(8,128)}, bf16[4,128,2048]{2,1,0:T(8,128)(2,1)}, bf16[4,128,2048]{2,1,0:T(8,128)(2,1)}, f32[1,2048]{1,0:T(1,128)}) custom-call(bf16[512,2048]{1,0:T(8,128)(2,1)} %get-tuple-element.18.refs_0_.refs_5_, bf16[512,2048]{1,0:T(8,128)(2,1)} %get-tuple-element.19.refs_1_, ...), custom_call_target="tpu_custom_call" | custom-call | tf_op jit(solution)/shard_map/pallas_call | solution.py:553
  193.0 0.0 copy-done.1
  193.0 0.0 copy-done.2
  193.0 0.0 copy-done.9
  193.0 0.0 copy-start
  193.0 0.0 copy-start.3
  193.0 0.0 copy-start.8
  193.0 3.9 %fusion = (f32[128]{0:T(128)S(1)}, f32[128]{0:T(128)S(1)}, bf16[128,2048]{1,0:T(8,128)(2,1)}) fusion(bf16[128,2048]{1,0:T(8,128)(2,1)S(1)} %copy-done.1, f32[2048]{0:T(1024)S(1)} %copy-done.9, bf16[4,128,2048]{2,1,0:T(8,128)(2,1)} %get-tuple-element.26, bf16[4,128,2048]{2,1,0:T(8,128)(2,1)} %get-tuple-element.25, bf16[128,2048]{1,0:T(8,128)(2,1)S(1)} %copy-done.2), kind=kLoop, calls=%fused_computation.3 | loop fusion | flops 6291200 | bytes 5776384 | tf_op jit(solution)/shard_map/reduce_sum | solution.py:637
  196.9 0.0 copy-start.10
  196.9 0.0 copy-start.11
  197.0 0.0 copy-start.4
  197.0 0.0 copy-start.5
  197.0 0.0 copy-start.6
  197.0 0.0 copy-start.7
  197.0 0.0 copy-done
  197.0 0.0 copy-done.3
  197.0 1.4 fusion.3
  198.4 0.0 copy-done.10
  198.4 0.0 copy-done.11
  198.4 0.6 add.75
  199.0 0.0 copy-done.8
  199.0 0.0 copy-done.4
  199.0 0.0 copy-done.5
  199.0 0.0 copy-done.6
  199.0 0.1 copy-done.7
  199.1 1.4 bitcast_add_fusion.2
  (2 shorter events, 0.0 us)
Async XLA Ops:
  96.6 96.4 %copy-start.1 = (bf16[128,2048]{1,0:T(8,128)(2,1)S(1)}, bf16[128,2048]{1,0:T(8,128)(2,1)}, u32[]{:S(2)}) copy-start(bf16[128,2048]{1,0:T(8,128)(2,1)} %refs_4_.1) | copy-start | bytes 1572868
  96.6 96.4 %copy-start.2 = (bf16[128,2048]{1,0:T(8,128)(2,1)S(1)}, bf16[128,2048]{1,0:T(8,128)(2,1)}, u32[]{:S(2)}) copy-start(bf16[128,2048]{1,0:T(8,128)(2,1)} %refs_3_.1) | copy-start | bytes 1572868
  96.6 96.4 %copy-start.9 = (f32[2048]{0:T(1024)S(1)}, f32[2048]{0:T(1024)}, u32[]{:S(2)}) copy-start(f32[2048]{0:T(1024)} %convert_element_type.51) | copy-start | bytes 24580
  193.0 4.0 %copy-start = (bf16[4,128,2048]{2,1,0:T(8,128)(2,1)S(1)}, bf16[4,128,2048]{2,1,0:T(8,128)(2,1)}, u32[]{:S(2)}) copy-start(bf16[4,128,2048]{2,1,0:T(8,128)(2,1)} %get-tuple-element.26) | copy-start | bytes 6291460
  193.0 4.0 %copy-start.3 = (bf16[128,2048]{1,0:T(8,128)(2,1)S(1)}, bf16[128,2048]{1,0:T(8,128)(2,1)}, u32[]{:S(2)}) copy-start(bf16[128,2048]{1,0:T(8,128)(2,1)} %refs_5_.1) | copy-start | bytes 1572868
  193.0 6.0 %copy-start.8 = (f32[704,256]{1,0:T(8,128)S(1)}, f32[704,256]{1,0:T(8,128)}, u32[]{:S(2)}) copy-start(f32[704,256]{1,0:T(8,128)} %get-tuple-element.28) | copy-start | bytes 2162692
  196.9 1.5 copy-start.10
  196.9 1.5 copy-start.11
  197.0 2.1 %copy-start.4 = (f32[1408,256]{1,0:T(8,128)S(1)}, f32[1408,256]{1,0:T(8,128)}, u32[]{:S(2)}) copy-start(f32[1408,256]{1,0:T(8,128)} %get-tuple-element.27) | copy-start | bytes 4325380
  197.0 2.1 %copy-start.5 = (f32[256,704]{0,1:T(8,128)S(1)}, f32[256,704]{0,1:T(8,128)}, u32[]{:S(2)}) copy-start(f32[256,704]{0,1:T(8,128)} %param.19) | copy-start | bytes 2162692
  197.0 2.1 %copy-start.6 = (f32[256,704]{0,1:T(8,128)S(1)}, f32[256,704]{0,1:T(8,128)}, u32[]{:S(2)}) copy-start(f32[256,704]{0,1:T(8,128)} %param.18) | copy-start | bytes 2162692
  197.0 2.2 %copy-start.7 = (f32[256,704]{0,1:T(8,128)S(1)}, f32[256,704]{0,1:T(8,128)}, u32[]{:S(2)}) copy-start(f32[256,704]{0,1:T(8,128)} %param.20) | copy-start | bytes 2162692
